TPU v7x, 128 devices: a whole 4x4x4 slice. The times are simulated.
128 devices in a mesh: sp: 32 (over z, y, core), tp: 4 (over x).
Axes of the slice: x: 4, y: 4, z: 4, core: 2. Of those that a mesh axis runs over, the one named last changes fastest.
Arguments:
- tokens: bfloat16 [16384, 2048], P(('sp', 'tp')), may hold values from -6 to 6
- norm_gain: float32 [2048], replicated, may hold values from 0.1 to 1.9
- query_weight: bfloat16 [2048, 1024], P(None, 'tp'), may hold values from -0.13258252 to 0.13258252
- key_weight: bfloat16 [2048, 1024], P(None, 'tp'), may hold values from -0.13258252 to 0.13258252
- value_weight: bfloat16 [2048, 1024], P(None, 'tp'), may hold values from -0.125 to 0.125
- glu_value_weight: bfloat16 [2048, 1024], P(None, 'tp'), may hold values from -0.125 to 0.125
- glu_gate_weight: bfloat16 [2048, 1024], P(None, 'tp'), may hold values from -0.125 to 0.125
- qk_gain: float32 [2, 64], replicated, may hold values from 1 to 6
- mix_lambda: float32 [8], P('tp'), may hold values from 0.3 to 0.8
- head_gain: float32 [128], replicated, may hold values from 0.1 to 1.9
- conv_kernel: float32 [31, 1024], P(None, 'tp'), may hold values from -1 to 1
- channel_gain: float32 [1024], P('tp'), may hold values from 0.1 to 1.9
- channel_shift: float32 [1024], P('tp'), may hold values from -3 to 3
- output_weight: bfloat16 [2048, 2048], replicated, may hold values from -0.125 to 0.125
Outputs:
- mixed: bfloat16 [16384, 2048], P(('sp', 'tp'))
- log_totals: float32 [2, 8, 16384], P(None, 'tp', 'sp')
All inputs are finite; a program needn't handle non-finite values.
Results may differ from a plain program's by a relative error of at most 0.035.
Values may be sent and summed in bfloat16 or wider, within the bound.
A program may use at most 128 MiB of HBM per device.

v0:
```python
import math

import jax
import jax.numpy as jnp
from jax import lax
from jax.sharding import PartitionSpec as P


def joined_along(tiles, dim):
    dims = list(tiles.shape[1:])
    dims[dim] *= tiles.shape[0]
    return jnp.moveaxis(tiles, 0, dim).reshape(dims)


def sent_to_all(shard, axis):
    copies = jnp.broadcast_to(shard, (lax.axis_size(axis), *shard.shape))
    return lax.all_to_all(copies, axis, split_axis=0, concat_axis=0, tiled=True)


def collect(shard, axis, dim):
    return joined_along(sent_to_all(shard, axis), dim)


def from_behind(value, axis, steps):
    count = lax.axis_size(axis)
    leading, last = (max(0, -steps), min(count, count - steps))
    return lax.ppermute(value, axis, [(source, source + steps) for source in range(leading, last)])


def over_copies(shard, axis):
    everything = sent_to_all(shard, axis)
    return jnp.sum(everything, axis=0)


def in_one(arrays, axis):
    ends = [0]
    for a in arrays:
        ends.append(ends[-1] + a.size)
    total = over_copies(jnp.concatenate([a.ravel() for a in arrays]), axis)
    return tuple((total[b:e].reshape(a.shape) for a, b, e in zip(arrays, ends, ends[1:])))


def rotate(values, positions):
    half = values.shape[-1] // 2
    inverse = 10000.0 ** (-jnp.arange(0, half, dtype=jnp.float32) * 2.0 / values.shape[-1])
    angles = positions[:, None] * inverse[None, :]
    cosine = jnp.cos(angles)[:, None, None, :]
    sine = jnp.sin(angles)[:, None, None, :]
    first = values[..., :half]
    second = values[..., half:]
    return jnp.concatenate(
        [first * cosine - second * sine, second * cosine + first * sine], axis=-1
    )


def prepare(raw, qk_gain, positions):
    values = raw.astype(jnp.float32)
    values = values * lax.rsqrt(jnp.mean(values * values, axis=-1, keepdims=True) + 1e-06)
    values = values * qk_gain[None, None, :, :]
    return rotate(values, positions).astype(jnp.bfloat16)


def per_device(
    tokens,
    norm_gain,
    query_weight,
    key_weight,
    value_weight,
    glu_value_weight,
    glu_gate_weight,
    qk_gain,
    mix_lambda,
    head_gain,
    conv_kernel,
    channel_gain,
    channel_shift,
    output_weight,
):
    head_size = qk_gain.shape[1]
    heads_here = mix_lambda.shape[0]
    value_size = head_gain.shape[0]
    kernel_len = conv_kernel.shape[0]
    conv_here = conv_kernel.shape[1]
    width = tokens.shape[1]
    matrices = (query_weight, key_weight, value_weight, glu_value_weight, glu_gate_weight)

    def project(piece):
        inputs = piece.astype(jnp.float32)
        normed = (
            inputs
            * lax.rsqrt(jnp.mean(inputs * inputs, axis=-1, keepdims=True) + 1e-06)
            * norm_gain
        ).astype(jnp.bfloat16)
        results = [
            jnp.dot(normed, matrix, preferred_element_type=jnp.float32).astype(jnp.bfloat16)
            for matrix in matrices
        ]
        return jnp.concatenate(results, axis=1)

    projected = project(collect(tokens, "tp", 0))
    tok_rows = projected.shape[0]
    bounds = [0]
    for matrix in matrices:
        bounds.append(bounds[-1] + matrix.shape[1])
    queries = projected[:, bounds[0] : bounds[1]].reshape(tok_rows, heads_here, 2, head_size)
    keys = projected[:, bounds[1] : bounds[2]].reshape(tok_rows, heads_here, 2, head_size)
    values = projected[:, bounds[2] : bounds[3]].reshape(tok_rows, heads_here, value_size)
    glu_a = projected[:, bounds[3] : bounds[4]]
    glu_g = projected[:, bounds[4] : bounds[5]]
    offset = lax.axis_index("sp") * tok_rows
    query_pos = offset + jnp.arange(tok_rows, dtype=jnp.int32)
    float_pos = query_pos.astype(jnp.float32)
    rq = jnp.transpose(prepare(queries, qk_gain, float_pos), (1, 2, 0, 3))
    rk = prepare(keys, qk_gain, float_pos)
    scale = head_size ** (-0.5)
    last_query = offset + tok_rows - 1
    initial = (
        jnp.full((heads_here, 2, tok_rows), -1e30, jnp.float32),
        jnp.zeros((heads_here, 2, tok_rows), jnp.float32),
        jnp.zeros((heads_here, 2, tok_rows, value_size), jnp.float32),
    )
    carry = initial
    key_piece = lax.all_gather(rk, "sp", axis=0, tiled=True)
    value_piece = lax.all_gather(values, "sp", axis=0, tiled=True)
    count = key_piece.shape[0]
    block = math.gcd(count, 512)
    blocks = count // block
    key_blocks = key_piece.reshape(blocks, block, heads_here, 2, head_size)
    value_blocks = value_piece.reshape(blocks, block, heads_here, value_size)

    def advance(state, item):
        key_block, value_block, number = item
        key_start = number * block

        def compute(inner):
            running, totals, summed = inner
            scores = (
                jnp.einsum("hmqd,khmd->hmqk", rq, key_block, preferred_element_type=jnp.float32)
                * scale
            )
            key_pos = key_start + jnp.arange(block, dtype=jnp.int32)
            allowed = key_pos[None, :] <= query_pos[:, None]
            scores = jnp.where(allowed[None, None], scores, -1e30)
            newtop = jnp.maximum(running, jnp.max(scores, axis=-1))
            probs = jnp.where(allowed[None, None], jnp.exp(scores - newtop[..., None]), 0.0)
            factor = jnp.exp(running - newtop)
            totals = totals * factor + jnp.sum(probs, axis=-1)
            added = jnp.einsum(
                "hmqk,khd->hmqd",
                probs.astype(jnp.bfloat16),
                value_block,
                preferred_element_type=jnp.float32,
            )
            return (newtop, totals, summed * factor[..., None] + added)

        def keep(inner):
            return inner

        return (lax.cond(key_start <= last_query, compute, keep, state), None)

    carry, unused = lax.scan(
        advance, carry, (key_blocks, value_blocks, jnp.arange(blocks, dtype=jnp.int32))
    )
    running, totals, summed = carry
    heads_out = (
        summed[:, 0] / totals[:, 0, :, None]
        - mix_lambda[:, None, None] * summed[:, 1] / totals[:, 1, :, None]
    )
    heads_out = (
        heads_out
        * lax.rsqrt(jnp.mean(heads_out * heads_out, axis=-1, keepdims=True) + 1e-06)
        * head_gain
    )
    attended = jnp.transpose(heads_out.astype(jnp.bfloat16), (1, 0, 2)).reshape(
        tok_rows, heads_here * value_size
    )
    log_totals = jnp.transpose(running + jnp.log(totals), (1, 0, 2))
    gated = (glu_a.astype(jnp.float32) * jax.nn.sigmoid(glu_g.astype(jnp.float32))).astype(
        jnp.bfloat16
    )
    earlier = from_behind(gated[tok_rows - (kernel_len - 1) :], "sp", 1)
    extended = jnp.concatenate([earlier, gated], axis=0).astype(jnp.float32)
    convolved = jnp.zeros((tok_rows, conv_here), jnp.float32)
    for step in range(kernel_len):
        convolved = convolved + conv_kernel[step][None, :] * extended[step : step + tok_rows]
    plain_sum, square_sum = in_one(
        (jnp.sum(convolved, axis=1), jnp.sum(convolved * convolved, axis=1)), "tp"
    )
    channels = conv_here * lax.axis_size("tp")
    middle = (plain_sum / channels)[:, None]
    spread = (square_sum / channels)[:, None] - middle * middle
    conv_out = jax.nn.silu(
        (convolved - middle) * lax.rsqrt(spread + 1e-05) * channel_gain + channel_shift
    ).astype(jnp.bfloat16)
    merged = jnp.concatenate([attended, conv_out], axis=1)
    groups = lax.axis_size("tp")
    branch_width = heads_here * value_size
    weight_view = output_weight.reshape(2, groups, branch_width, width)
    moved = lax.all_to_all(merged, "tp", split_axis=0, concat_axis=1, tiled=True)
    arranged = moved.reshape(tok_rows // groups, groups, 2, branch_width)
    mixed = jnp.einsum(
        "rtcj,ctjd->rd", arranged, weight_view, preferred_element_type=jnp.float32
    ).astype(jnp.bfloat16)
    return (mixed, log_totals)


def solution(mesh):
    placed = (
        P(("sp", "tp"), None),
        P(),
        P(None, "tp"),
        P(None, "tp"),
        P(None, "tp"),
        P(None, "tp"),
        P(None, "tp"),
        P(),
        P("tp"),
        P(),
        P(None, "tp"),
        P("tp"),
        P("tp"),
        P(),
    )
    return jax.shard_map(
        per_device,
        mesh=mesh,
        in_specs=placed,
        out_specs=(P(("sp", "tp"), None), P(None, "tp", "sp")),
        check_vma=False,
    )
```

profile of v0, /device:TPU:121, one launch (start us, length us, event | category | flops | bytes accessed | tf_op | source)
XLA Modules:
  0.0 416.1 jit_solution(1099823068784679302)
XLA Ops:
  7.2 2.7 broadcast_in_dim.44
  9.9 4.0 all-to-all-start
  14.3 25.1 %all-to-all-done = bf16[4,128,2048]{2,1,0:T(8,128)(2,1)S(1)} async-done(((bf16[4,128,2048]{2,1,0:T(8,128)(2,1)}), bf16[4,128,2048]{2,1,0:T(8,128)(2,1)S(1)}, u32[]{:S(2)}, u32[]{:S(2)}) %all-to-all-start) | async-done | bytes 2097184 | tf_op jit(solution)/shard_map/all_to_all | solution.py:17
  58.0 3.4 all-to-all-start.1
  61.4 4.0 all-to-all-done.1
  65.8 35.1 %all-gather.3.cloned.1.call-done = bf16[16384,2,2,64]{0,3,2,1:T(8,128)(2,1)} async-done(((bf16[512,2,2,64]{0,3,2,1:T(8,128)(2,1)}), bf16[16384,2,2,64]{0,3,2,1:T(8,128)(2,1)}) %all-gather.3.cloned.1.call-update) | async-done | bytes 8388624 | tf_op jit(solution)/shard_map/all_gather | solution.py:123
  100.9 7.9 %copy.75 = bf16[2,2,8,32,8,512]{5,4,2,1,0,3:T(8,128)(2,1)} copy(bf16[2,2,8,32,8,512]{5,4,3,2,1,0:T(8,128)(2,1)} %bitcast.129) | data formatting | bytes 16777216 | tf_op jit(solution)/shard_map/reshape | solution.py:128
  108.8 46.9 %all-gather.5.cloned.1.call-done = bf16[16384,2,128]{2,0,1:T(8,128)(2,1)} async-done(((bf16[512,2,128]{2,0,1:T(8,128)(2,1)}), bf16[16384,2,128]{2,0,1:T(8,128)(2,1)}) %all-gather.5.cloned.1.call-update) | async-done | bytes 8388624 | tf_op jit(solution)/shard_map/all_gather | solution.py:124
  155.6 7.6 %copy.43 = bf16[32,512,2,128]{3,1,2,0:T(8,128)(2,1)} copy(bf16[32,512,2,128]{3,1,0,2:T(8,128)(2,1)} %bitcast.130) | data formatting | bytes 16777216
  163.4 227.0 %while.15 = (s32[]{:T(128)}, f32[2,2,512]{2,1,0:T(2,128)S(1)}, f32[2,2,512]{2,1,0:T(2,128)S(1)}, f32[2,2,512,128]{3,2,1,0:T(8,128)S(1)}, s32[32]{0:T(128)S(1)}, ...) while((s32[]{:T(128)}, f32[2,2,512]{2,1,0:T(2,128)S(1)}, ...), condition=%wide.region_8.9_spmd.clone, body=%wide.region_3.8_spmd.clone.sunk | while | flops 417076224 | bytes 16659763 | solution.py:161
  164.5 5.9 %conditional.3 = ((f32[2,2,512]{2,1,0:T(2,128)S(1)}, f32[2,2,512]{2,1,0:T(2,128)S(1)}, f32[2,2,512,128]{3,2,1,0:T(8,128)S(1)})) conditional(s32[]{:T(128)} %convert_element_type.153, (f32[2,2,512]{2,1,0:T(2,128)S(1)}, f32[2,2,512]{2,1,0:T(2,128)S(1)}, f32[2,2,512,128]{3,2,1,0:T(8,128)S(1)}) %tuple.89, (s32[]{:T(128)}, s32[]{:T(128)}, ...), branch_computations={%region_4.4_spmd, %region_5.7_spmd} | conditional | flops 417076224 | bytes 16657448 | solution.py:159
  167.7 2.7 fusion.8
  171.6 5.9 %conditional.3 = ((f32[2,2,512]{2,1,0:T(2,128)S(1)}, f32[2,2,512]{2,1,0:T(2,128)S(1)}, f32[2,2,512,128]{3,2,1,0:T(8,128)S(1)})) conditional(s32[]{:T(128)} %convert_element_type.153, (f32[2,2,512]{2,1,0:T(2,128)S(1)}, f32[2,2,512]{2,1,0:T(2,128)S(1)}, f32[2,2,512,128]{3,2,1,0:T(8,128)S(1)}) %tuple.89, (s32[]{:T(128)}, s32[]{:T(128)}, ...), branch_computations={%region_4.4_spmd, %region_5.7_spmd} | conditional | flops 417076224 | bytes 16657448 | solution.py:159
  178.7 5.9 %conditional.3 = ((f32[2,2,512]{2,1,0:T(2,128)S(1)}, f32[2,2,512]{2,1,0:T(2,128)S(1)}, f32[2,2,512,128]{3,2,1,0:T(8,128)S(1)})) conditional(s32[]{:T(128)} %convert_element_type.153, (f32[2,2,512]{2,1,0:T(2,128)S(1)}, f32[2,2,512]{2,1,0:T(2,128)S(1)}, f32[2,2,512,128]{3,2,1,0:T(8,128)S(1)}) %tuple.89, (s32[]{:T(128)}, s32[]{:T(128)}, ...), branch_computations={%region_4.4_spmd, %region_5.7_spmd} | conditional | flops 417076224 | bytes 16657448 | solution.py:159
  185.8 5.9 %conditional.3 = ((f32[2,2,512]{2,1,0:T(2,128)S(1)}, f32[2,2,512]{2,1,0:T(2,128)S(1)}, f32[2,2,512,128]{3,2,1,0:T(8,128)S(1)})) conditional(s32[]{:T(128)} %convert_element_type.153, (f32[2,2,512]{2,1,0:T(2,128)S(1)}, f32[2,2,512]{2,1,0:T(2,128)S(1)}, f32[2,2,512,128]{3,2,1,0:T(8,128)S(1)}) %tuple.89, (s32[]{:T(128)}, s32[]{:T(128)}, ...), branch_computations={%region_4.4_spmd, %region_5.7_spmd} | conditional | flops 417076224 | bytes 16657448 | solution.py:159
  192.9 5.9 %conditional.3 = ((f32[2,2,512]{2,1,0:T(2,128)S(1)}, f32[2,2,512]{2,1,0:T(2,128)S(1)}, f32[2,2,512,128]{3,2,1,0:T(8,128)S(1)})) conditional(s32[]{:T(128)} %convert_element_type.153, (f32[2,2,512]{2,1,0:T(2,128)S(1)}, f32[2,2,512]{2,1,0:T(2,128)S(1)}, f32[2,2,512,128]{3,2,1,0:T(8,128)S(1)}) %tuple.89, (s32[]{:T(128)}, s32[]{:T(128)}, ...), branch_computations={%region_4.4_spmd, %region_5.7_spmd} | conditional | flops 417076224 | bytes 16657448 | solution.py:159
  200.0 5.9 %conditional.3 = ((f32[2,2,512]{2,1,0:T(2,128)S(1)}, f32[2,2,512]{2,1,0:T(2,128)S(1)}, f32[2,2,512,128]{3,2,1,0:T(8,128)S(1)})) conditional(s32[]{:T(128)} %convert_element_type.153, (f32[2,2,512]{2,1,0:T(2,128)S(1)}, f32[2,2,512]{2,1,0:T(2,128)S(1)}, f32[2,2,512,128]{3,2,1,0:T(8,128)S(1)}) %tuple.89, (s32[]{:T(128)}, s32[]{:T(128)}, ...), branch_computations={%region_4.4_spmd, %region_5.7_spmd} | conditional | flops 417076224 | bytes 16657448 | solution.py:159
  207.1 5.9 %conditional.3 = ((f32[2,2,512]{2,1,0:T(2,128)S(1)}, f32[2,2,512]{2,1,0:T(2,128)S(1)}, f32[2,2,512,128]{3,2,1,0:T(8,128)S(1)})) conditional(s32[]{:T(128)} %convert_element_type.153, (f32[2,2,512]{2,1,0:T(2,128)S(1)}, f32[2,2,512]{2,1,0:T(2,128)S(1)}, f32[2,2,512,128]{3,2,1,0:T(8,128)S(1)}) %tuple.89, (s32[]{:T(128)}, s32[]{:T(128)}, ...), branch_computations={%region_4.4_spmd, %region_5.7_spmd} | conditional | flops 417076224 | bytes 16657448 | solution.py:159
  214.2 5.9 %conditional.3 = ((f32[2,2,512]{2,1,0:T(2,128)S(1)}, f32[2,2,512]{2,1,0:T(2,128)S(1)}, f32[2,2,512,128]{3,2,1,0:T(8,128)S(1)})) conditional(s32[]{:T(128)} %convert_element_type.153, (f32[2,2,512]{2,1,0:T(2,128)S(1)}, f32[2,2,512]{2,1,0:T(2,128)S(1)}, f32[2,2,512,128]{3,2,1,0:T(8,128)S(1)}) %tuple.89, (s32[]{:T(128)}, s32[]{:T(128)}, ...), branch_computations={%region_4.4_spmd, %region_5.7_spmd} | conditional | flops 417076224 | bytes 16657448 | solution.py:159
  221.3 5.9 %conditional.3 = ((f32[2,2,512]{2,1,0:T(2,128)S(1)}, f32[2,2,512]{2,1,0:T(2,128)S(1)}, f32[2,2,512,128]{3,2,1,0:T(8,128)S(1)})) conditional(s32[]{:T(128)} %convert_element_type.153, (f32[2,2,512]{2,1,0:T(2,128)S(1)}, f32[2,2,512]{2,1,0:T(2,128)S(1)}, f32[2,2,512,128]{3,2,1,0:T(8,128)S(1)}) %tuple.89, (s32[]{:T(128)}, s32[]{:T(128)}, ...), branch_computations={%region_4.4_spmd, %region_5.7_spmd} | conditional | flops 417076224 | bytes 16657448 | solution.py:159
  228.4 5.9 %conditional.3 = ((f32[2,2,512]{2,1,0:T(2,128)S(1)}, f32[2,2,512]{2,1,0:T(2,128)S(1)}, f32[2,2,512,128]{3,2,1,0:T(8,128)S(1)})) conditional(s32[]{:T(128)} %convert_element_type.153, (f32[2,2,512]{2,1,0:T(2,128)S(1)}, f32[2,2,512]{2,1,0:T(2,128)S(1)}, f32[2,2,512,128]{3,2,1,0:T(8,128)S(1)}) %tuple.89, (s32[]{:T(128)}, s32[]{:T(128)}, ...), branch_computations={%region_4.4_spmd, %region_5.7_spmd} | conditional | flops 417076224 | bytes 16657448 | solution.py:159
  235.5 5.9 %conditional.3 = ((f32[2,2,512]{2,1,0:T(2,128)S(1)}, f32[2,2,512]{2,1,0:T(2,128)S(1)}, f32[2,2,512,128]{3,2,1,0:T(8,128)S(1)})) conditional(s32[]{:T(128)} %convert_element_type.153, (f32[2,2,512]{2,1,0:T(2,128)S(1)}, f32[2,2,512]{2,1,0:T(2,128)S(1)}, f32[2,2,512,128]{3,2,1,0:T(8,128)S(1)}) %tuple.89, (s32[]{:T(128)}, s32[]{:T(128)}, ...), branch_computations={%region_4.4_spmd, %region_5.7_spmd} | conditional | flops 417076224 | bytes 16657448 | solution.py:159
  242.6 5.9 %conditional.3 = ((f32[2,2,512]{2,1,0:T(2,128)S(1)}, f32[2,2,512]{2,1,0:T(2,128)S(1)}, f32[2,2,512,128]{3,2,1,0:T(8,128)S(1)})) conditional(s32[]{:T(128)} %convert_element_type.153, (f32[2,2,512]{2,1,0:T(2,128)S(1)}, f32[2,2,512]{2,1,0:T(2,128)S(1)}, f32[2,2,512,128]{3,2,1,0:T(8,128)S(1)}) %tuple.89, (s32[]{:T(128)}, s32[]{:T(128)}, ...), branch_computations={%region_4.4_spmd, %region_5.7_spmd} | conditional | flops 417076224 | bytes 16657448 | solution.py:159
  249.7 5.9 %conditional.3 = ((f32[2,2,512]{2,1,0:T(2,128)S(1)}, f32[2,2,512]{2,1,0:T(2,128)S(1)}, f32[2,2,512,128]{3,2,1,0:T(8,128)S(1)})) conditional(s32[]{:T(128)} %convert_element_type.153, (f32[2,2,512]{2,1,0:T(2,128)S(1)}, f32[2,2,512]{2,1,0:T(2,128)S(1)}, f32[2,2,512,128]{3,2,1,0:T(8,128)S(1)}) %tuple.89, (s32[]{:T(128)}, s32[]{:T(128)}, ...), branch_computations={%region_4.4_spmd, %region_5.7_spmd} | conditional | flops 417076224 | bytes 16657448 | solution.py:159
  256.7 5.9 %conditional.3 = ((f32[2,2,512]{2,1,0:T(2,128)S(1)}, f32[2,2,512]{2,1,0:T(2,128)S(1)}, f32[2,2,512,128]{3,2,1,0:T(8,128)S(1)})) conditional(s32[]{:T(128)} %convert_element_type.153, (f32[2,2,512]{2,1,0:T(2,128)S(1)}, f32[2,2,512]{2,1,0:T(2,128)S(1)}, f32[2,2,512,128]{3,2,1,0:T(8,128)S(1)}) %tuple.89, (s32[]{:T(128)}, s32[]{:T(128)}, ...), branch_computations={%region_4.4_spmd, %region_5.7_spmd} | conditional | flops 417076224 | bytes 16657448 | solution.py:159
  263.8 5.9 %conditional.3 = ((f32[2,2,512]{2,1,0:T(2,128)S(1)}, f32[2,2,512]{2,1,0:T(2,128)S(1)}, f32[2,2,512,128]{3,2,1,0:T(8,128)S(1)})) conditional(s32[]{:T(128)} %convert_element_type.153, (f32[2,2,512]{2,1,0:T(2,128)S(1)}, f32[2,2,512]{2,1,0:T(2,128)S(1)}, f32[2,2,512,128]{3,2,1,0:T(8,128)S(1)}) %tuple.89, (s32[]{:T(128)}, s32[]{:T(128)}, ...), branch_computations={%region_4.4_spmd, %region_5.7_spmd} | conditional | flops 417076224 | bytes 16657448 | solution.py:159
  270.9 5.9 %conditional.3 = ((f32[2,2,512]{2,1,0:T(2,128)S(1)}, f32[2,2,512]{2,1,0:T(2,128)S(1)}, f32[2,2,512,128]{3,2,1,0:T(8,128)S(1)})) conditional(s32[]{:T(128)} %convert_element_type.153, (f32[2,2,512]{2,1,0:T(2,128)S(1)}, f32[2,2,512]{2,1,0:T(2,128)S(1)}, f32[2,2,512,128]{3,2,1,0:T(8,128)S(1)}) %tuple.89, (s32[]{:T(128)}, s32[]{:T(128)}, ...), branch_computations={%region_4.4_spmd, %region_5.7_spmd} | conditional | flops 417076224 | bytes 16657448 | solution.py:159
  278.0 5.9 %conditional.3 = ((f32[2,2,512]{2,1,0:T(2,128)S(1)}, f32[2,2,512]{2,1,0:T(2,128)S(1)}, f32[2,2,512,128]{3,2,1,0:T(8,128)S(1)})) conditional(s32[]{:T(128)} %convert_element_type.153, (f32[2,2,512]{2,1,0:T(2,128)S(1)}, f32[2,2,512]{2,1,0:T(2,128)S(1)}, f32[2,2,512,128]{3,2,1,0:T(8,128)S(1)}) %tuple.89, (s32[]{:T(128)}, s32[]{:T(128)}, ...), branch_computations={%region_4.4_spmd, %region_5.7_spmd} | conditional | flops 417076224 | bytes 16657448 | solution.py:159
  285.1 5.9 %conditional.3 = ((f32[2,2,512]{2,1,0:T(2,128)S(1)}, f32[2,2,512]{2,1,0:T(2,128)S(1)}, f32[2,2,512,128]{3,2,1,0:T(8,128)S(1)})) conditional(s32[]{:T(128)} %convert_element_type.153, (f32[2,2,512]{2,1,0:T(2,128)S(1)}, f32[2,2,512]{2,1,0:T(2,128)S(1)}, f32[2,2,512,128]{3,2,1,0:T(8,128)S(1)}) %tuple.89, (s32[]{:T(128)}, s32[]{:T(128)}, ...), branch_computations={%region_4.4_spmd, %region_5.7_spmd} | conditional | flops 417076224 | bytes 16657448 | solution.py:159
  292.2 5.9 %conditional.3 = ((f32[2,2,512]{2,1,0:T(2,128)S(1)}, f32[2,2,512]{2,1,0:T(2,128)S(1)}, f32[2,2,512,128]{3,2,1,0:T(8,128)S(1)})) conditional(s32[]{:T(128)} %convert_element_type.153, (f32[2,2,512]{2,1,0:T(2,128)S(1)}, f32[2,2,512]{2,1,0:T(2,128)S(1)}, f32[2,2,512,128]{3,2,1,0:T(8,128)S(1)}) %tuple.89, (s32[]{:T(128)}, s32[]{:T(128)}, ...), branch_computations={%region_4.4_spmd, %region_5.7_spmd} | conditional | flops 417076224 | bytes 16657448 | solution.py:159
  299.3 5.9 %conditional.3 = ((f32[2,2,512]{2,1,0:T(2,128)S(1)}, f32[2,2,512]{2,1,0:T(2,128)S(1)}, f32[2,2,512,128]{3,2,1,0:T(8,128)S(1)})) conditional(s32[]{:T(128)} %convert_element_type.153, (f32[2,2,512]{2,1,0:T(2,128)S(1)}, f32[2,2,512]{2,1,0:T(2,128)S(1)}, f32[2,2,512,128]{3,2,1,0:T(8,128)S(1)}) %tuple.89, (s32[]{:T(128)}, s32[]{:T(128)}, ...), branch_computations={%region_4.4_spmd, %region_5.7_spmd} | conditional | flops 417076224 | bytes 16657448 | solution.py:159
  306.4 5.9 %conditional.3 = ((f32[2,2,512]{2,1,0:T(2,128)S(1)}, f32[2,2,512]{2,1,0:T(2,128)S(1)}, f32[2,2,512,128]{3,2,1,0:T(8,128)S(1)})) conditional(s32[]{:T(128)} %convert_element_type.153, (f32[2,2,512]{2,1,0:T(2,128)S(1)}, f32[2,2,512]{2,1,0:T(2,128)S(1)}, f32[2,2,512,128]{3,2,1,0:T(8,128)S(1)}) %tuple.89, (s32[]{:T(128)}, s32[]{:T(128)}, ...), branch_computations={%region_4.4_spmd, %region_5.7_spmd} | conditional | flops 417076224 | bytes 16657448 | solution.py:159
  309.6 2.7 fusion.8
  313.5 5.9 %conditional.3 = ((f32[2,2,512]{2,1,0:T(2,128)S(1)}, f32[2,2,512]{2,1,0:T(2,128)S(1)}, f32[2,2,512,128]{3,2,1,0:T(8,128)S(1)})) conditional(s32[]{:T(128)} %convert_element_type.153, (f32[2,2,512]{2,1,0:T(2,128)S(1)}, f32[2,2,512]{2,1,0:T(2,128)S(1)}, f32[2,2,512,128]{3,2,1,0:T(8,128)S(1)}) %tuple.89, (s32[]{:T(128)}, s32[]{:T(128)}, ...), branch_computations={%region_4.4_spmd, %region_5.7_spmd} | conditional | flops 417076224 | bytes 16657448 | solution.py:159
  320.6 5.9 %conditional.3 = ((f32[2,2,512]{2,1,0:T(2,128)S(1)}, f32[2,2,512]{2,1,0:T(2,128)S(1)}, f32[2,2,512,128]{3,2,1,0:T(8,128)S(1)})) conditional(s32[]{:T(128)} %convert_element_type.153, (f32[2,2,512]{2,1,0:T(2,128)S(1)}, f32[2,2,512]{2,1,0:T(2,128)S(1)}, f32[2,2,512,128]{3,2,1,0:T(8,128)S(1)}) %tuple.89, (s32[]{:T(128)}, s32[]{:T(128)}, ...), branch_computations={%region_4.4_spmd, %region_5.7_spmd} | conditional | flops 417076224 | bytes 16657448 | solution.py:159
  323.8 2.7 fusion.8
  327.7 5.9 %conditional.3 = ((f32[2,2,512]{2,1,0:T(2,128)S(1)}, f32[2,2,512]{2,1,0:T(2,128)S(1)}, f32[2,2,512,128]{3,2,1,0:T(8,128)S(1)})) conditional(s32[]{:T(128)} %convert_element_type.153, (f32[2,2,512]{2,1,0:T(2,128)S(1)}, f32[2,2,512]{2,1,0:T(2,128)S(1)}, f32[2,2,512,128]{3,2,1,0:T(8,128)S(1)}) %tuple.89, (s32[]{:T(128)}, s32[]{:T(128)}, ...), branch_computations={%region_4.4_spmd, %region_5.7_spmd} | conditional | flops 417076224 | bytes 16657448 | solution.py:159
  334.8 5.9 %conditional.3 = ((f32[2,2,512]{2,1,0:T(2,128)S(1)}, f32[2,2,512]{2,1,0:T(2,128)S(1)}, f32[2,2,512,128]{3,2,1,0:T(8,128)S(1)})) conditional(s32[]{:T(128)} %convert_element_type.153, (f32[2,2,512]{2,1,0:T(2,128)S(1)}, f32[2,2,512]{2,1,0:T(2,128)S(1)}, f32[2,2,512,128]{3,2,1,0:T(8,128)S(1)}) %tuple.89, (s32[]{:T(128)}, s32[]{:T(128)}, ...), branch_computations={%region_4.4_spmd, %region_5.7_spmd} | conditional | flops 417076224 | bytes 16657448 | solution.py:159
  341.9 5.9 %conditional.3 = ((f32[2,2,512]{2,1,0:T(2,128)S(1)}, f32[2,2,512]{2,1,0:T(2,128)S(1)}, f32[2,2,512,128]{3,2,1,0:T(8,128)S(1)})) conditional(s32[]{:T(128)} %convert_element_type.153, (f32[2,2,512]{2,1,0:T(2,128)S(1)}, f32[2,2,512]{2,1,0:T(2,128)S(1)}, f32[2,2,512,128]{3,2,1,0:T(8,128)S(1)}) %tuple.89, (s32[]{:T(128)}, s32[]{:T(128)}, ...), branch_computations={%region_4.4_spmd, %region_5.7_spmd} | conditional | flops 417076224 | bytes 16657448 | solution.py:159
  349.0 5.9 %conditional.3 = ((f32[2,2,512]{2,1,0:T(2,128)S(1)}, f32[2,2,512]{2,1,0:T(2,128)S(1)}, f32[2,2,512,128]{3,2,1,0:T(8,128)S(1)})) conditional(s32[]{:T(128)} %convert_element_type.153, (f32[2,2,512]{2,1,0:T(2,128)S(1)}, f32[2,2,512]{2,1,0:T(2,128)S(1)}, f32[2,2,512,128]{3,2,1,0:T(8,128)S(1)}) %tuple.89, (s32[]{:T(128)}, s32[]{:T(128)}, ...), branch_computations={%region_4.4_spmd, %region_5.7_spmd} | conditional | flops 417076224 | bytes 16657448 | solution.py:159
  356.1 5.9 %conditional.3 = ((f32[2,2,512]{2,1,0:T(2,128)S(1)}, f32[2,2,512]{2,1,0:T(2,128)S(1)}, f32[2,2,512,128]{3,2,1,0:T(8,128)S(1)})) conditional(s32[]{:T(128)} %convert_element_type.153, (f32[2,2,512]{2,1,0:T(2,128)S(1)}, f32[2,2,512]{2,1,0:T(2,128)S(1)}, f32[2,2,512,128]{3,2,1,0:T(8,128)S(1)}) %tuple.89, (s32[]{:T(128)}, s32[]{:T(128)}, ...), branch_computations={%region_4.4_spmd, %region_5.7_spmd} | conditional | flops 417076224 | bytes 16657448 | solution.py:159
  363.2 5.9 %conditional.3 = ((f32[2,2,512]{2,1,0:T(2,128)S(1)}, f32[2,2,512]{2,1,0:T(2,128)S(1)}, f32[2,2,512,128]{3,2,1,0:T(8,128)S(1)})) conditional(s32[]{:T(128)} %convert_element_type.153, (f32[2,2,512]{2,1,0:T(2,128)S(1)}, f32[2,2,512]{2,1,0:T(2,128)S(1)}, f32[2,2,512,128]{3,2,1,0:T(8,128)S(1)}) %tuple.89, (s32[]{:T(128)}, s32[]{:T(128)}, ...), branch_computations={%region_4.4_spmd, %region_5.7_spmd} | conditional | flops 417076224 | bytes 16657448 | solution.py:159
  370.3 5.9 %conditional.3 = ((f32[2,2,512]{2,1,0:T(2,128)S(1)}, f32[2,2,512]{2,1,0:T(2,128)S(1)}, f32[2,2,512,128]{3,2,1,0:T(8,128)S(1)})) conditional(s32[]{:T(128)} %convert_element_type.153, (f32[2,2,512]{2,1,0:T(2,128)S(1)}, f32[2,2,512]{2,1,0:T(2,128)S(1)}, f32[2,2,512,128]{3,2,1,0:T(8,128)S(1)}) %tuple.89, (s32[]{:T(128)}, s32[]{:T(128)}, ...), branch_computations={%region_4.4_spmd, %region_5.7_spmd} | conditional | flops 417076224 | bytes 16657448 | solution.py:159
  377.4 5.9 %conditional.3 = ((f32[2,2,512]{2,1,0:T(2,128)S(1)}, f32[2,2,512]{2,1,0:T(2,128)S(1)}, f32[2,2,512,128]{3,2,1,0:T(8,128)S(1)})) conditional(s32[]{:T(128)} %convert_element_type.153, (f32[2,2,512]{2,1,0:T(2,128)S(1)}, f32[2,2,512]{2,1,0:T(2,128)S(1)}, f32[2,2,512,128]{3,2,1,0:T(8,128)S(1)}) %tuple.89, (s32[]{:T(128)}, s32[]{:T(128)}, ...), branch_computations={%region_4.4_spmd, %region_5.7_spmd} | conditional | flops 417076224 | bytes 16657448 | solution.py:159
  384.5 5.9 %conditional.3 = ((f32[2,2,512]{2,1,0:T(2,128)S(1)}, f32[2,2,512]{2,1,0:T(2,128)S(1)}, f32[2,2,512,128]{3,2,1,0:T(8,128)S(1)})) conditional(s32[]{:T(128)} %convert_element_type.153, (f32[2,2,512]{2,1,0:T(2,128)S(1)}, f32[2,2,512]{2,1,0:T(2,128)S(1)}, f32[2,2,512,128]{3,2,1,0:T(8,128)S(1)}) %tuple.89, (s32[]{:T(128)}, s32[]{:T(128)}, ...), branch_computations={%region_4.4_spmd, %region_5.7_spmd} | conditional | flops 417076224 | bytes 16657448 | solution.py:159
  392.5 4.0 all-to-all-start.2
  397.1 6.3 %all-to-all-done.2 = bf16[4,128,512]{2,1,0:T(8,128)(2,1)S(1)} async-done(((bf16[4,128,512]{2,1,0:T(8,128)(2,1)}), bf16[4,128,512]{2,1,0:T(8,128)(2,1)S(1)}, u32[]{:S(2)}, u32[]{:S(2)}) %all-to-all-start.2) | async-done | bytes 524320 | tf_op jit(solution)/shard_map/all_to_all | solution.py:199
  403.7 5.5 %fusion.23 = bf16[128,2048]{1,0:T(8,128)(2,1)} fusion(bf16[2,4,256,2048]{3,2,1,0:T(8,128)(2,1)} %bitcast.128, bf16[128,4,2,256]{0,3,2,1:T(8,128)(2,1)S(1)} %bitcast.132), kind=kOutput, calls=%fused_computation.30 | convolution fusion | flops 1074003968 | bytes 9437184 | tf_op jit(solution)/shard_map/rtcj,ctjd->rd/dot_general | solution.py:201
  (389 shorter events, 219.9 us)
Async XLA Ops:
  7.2 33.3 %copy-start = (bf16[2048,256]{1,0:T(8,128)(2,1)S(1)}, bf16[2048,256]{1,0:T(8,128)(2,1)}, u32[]{:S(2)}) copy-start(bf16[2048,256]{1,0:T(8,128)(2,1)} %param.20) | copy-start | bytes 3145732
  7.2 32.7 %copy-start.4 = (f32[2048]{0:T(1024)S(1)}, f32[2048]{0:T(1024)}, u32[]{:S(2)}) copy-start(f32[2048]{0:T(1024)} %param.19) | copy-start | bytes 24580
  9.9 29.5 %all-to-all-start = ((bf16[4,128,2048]{2,1,0:T(8,128)(2,1)}), bf16[4,128,2048]{2,1,0:T(8,128)(2,1)S(1)}, u32[]{:S(2)}, u32[]{:S(2)}) async-start(bf16[4,128,2048]{2,1,0:T(8,128)(2,1)} %broadcast_in_dim.44), calls=%async_computation | async-start | bytes 4194304 | tf_op jit(solution)/shard_map/all_to_all | solution.py:17
  13.9 86.9 %all-gather.3.cloned.1.call-start = ((), (), s32[]{:S(2)}) async-start(), calls=%async_computation.3 | async-start | bytes 8650752 | tf_op jit(solution)/shard_map/all_gather | solution.py:123
  39.9 1.4 copy-start.10
  40.5 1.8 copy-start.2
  40.5 1.6 copy-start.7
  42.3 5.5 %copy-start.3 = (bf16[512,2048]{1,0:T(8,128)(2,1)S(1)}, bf16[512,2048]{1,0:T(8,128)(2,1)}, u32[]{:S(2)}) copy-start(bf16[512,2048]{1,0:T(8,128)(2,1)} %copy-done.2) | copy-start | bytes 6291460
  43.2 112.4 %all-gather.5.cloned.1.call-start = ((), (), s32[]{:S(2)}) async-start(), calls=%async_computation.4 | async-start | bytes 8650752 | tf_op jit(solution)/shard_map/all_gather | solution.py:124
  46.7 3.0 copy-start.11
  50.5 4.4 %collective-permute-start = (bf16[30,256]{1,0:T(8,128)(2,1)S(1)}, bf16[30,256]{1,0:T(8,128)(2,1)S(1)}, u32[]{:S(2)}, u32[]{:S(2)}) collective-permute-start(bf16[30,256]{1,0:T(8,128)(2,1)S(1)} %slice.297), channel_id=1, source_target_pairs={{0,4},{4,8},{8,12},{12,16},{16,20},{20,24},{24,28},{28,32},{32,36}... | collective-permute-start | bytes 46088 | tf_op jit(solution)/shard_map/ppermute | solution.py:27
  54.9 10.6 %copy-start.5 = (f32[256]{0:T(256)S(1)}, f32[256]{0:T(256)}, u32[]{:S(2)}) copy-start(f32[256]{0:T(256)} %param.30) | copy-start | bytes 3076
  55.0 10.6 %copy-start.6 = (f32[256]{0:T(256)S(1)}, f32[256]{0:T(256)}, u32[]{:S(2)}) copy-start(f32[256]{0:T(256)} %param.29) | copy-start | bytes 3076
  58.0 7.5 %all-to-all-start.1 = ((f32[4,1,1024]{2,1,0:T(1,128)}), f32[4,1,1024]{2,1,0:T(1,128)S(1)}, u32[]{:S(2)}, u32[]{:S(2)}) async-start(f32[4,1,1024]{2,1,0:T(1,128)} %broadcast_in_dim.45), calls=%async_computation.1 | async-start | bytes 32768 | tf_op jit(solution)/shard_map/all_to_all | solution.py:17
  163.4 227.1 %copy-start.8 = (f32[2]{0:T(128)S(1)}, f32[2]{0:T(128)}, u32[]{:S(2)}) copy-start(f32[2]{0:T(128)} %param.26) | copy-start | bytes 28
  163.4 227.6 %copy-start.9 = (f32[128]{0:T(128)S(1)}, f32[128]{0:T(128)}, u32[]{:S(2)}) copy-start(f32[128]{0:T(128)} %param.27) | copy-start | bytes 1540
  392.5 10.9 %all-to-all-start.2 = ((bf16[4,128,512]{2,1,0:T(8,128)(2,1)}), bf16[4,128,512]{2,1,0:T(8,128)(2,1)S(1)}, u32[]{:S(2)}, u32[]{:S(2)}) async-start(bf16[4,128,512]{2,1,0:T(8,128)(2,1)} %pad_maximum_fusion), calls=%async_computation.2 | async-start | bytes 1048576 | tf_op jit(solution)/shard_map/all_to_all | solution.py:199
  403.7 5.6 %copy-start.1 = (bf16[2048,256]{1,0:T(8,128)(2,1)S(1)}, bf16[2048,256]{1,0:T(8,128)(2,1)}, u32[]{:S(2)}) copy-start(bf16[2048,256]{1,0:T(8,128)(2,1)} %param.20) | copy-start | bytes 3145732
Sparse Core Ops, SparseCore 0:
  43.3 57.4 all-gather.2
  103.2 52.4 all-gather.4
where the time goes:
time: 419 us; the launch traced here: 416 us
  matrix products  159 us (38%)
  waiting for transfers between devices  120 us (29%)
  other arithmetic  48.7 us (12%)
  local copies, waits for them, and re-layouts  40.6 us (10%)
  loops' own time  21 us (5%)
  between operations  14.4 us (3%)
  starting transfers between devices  12.7 us (3%)
    dot_general x32, matrix products, compute(): jnp.einsum('hmqk,khd->hmqd', probs.astype(jnp.bfloat16), value_block, pre...  87.2 us
    dot_general x32, matrix products, compute(): jnp.einsum('hmqd,khmd->hmqk', rq, key_block, preferred_element_type=jnp.f...  59.5 us
    all_gather x1, waiting for transfers between devices, per_device(): value_piece = lax.all_gather(values, 'sp', axis=0, tiled=True)  46.9 us
    all_gather x1, waiting for transfers between devices, per_device(): key_piece = lax.all_gather(rk, 'sp', axis=0, tiled=True)  35.1 us
    reduce_sum x32, other arithmetic, compute(): totals = totals * factor + jnp.sum(probs, axis=-1)  33.3 us
    all_to_all x2, waiting for transfers between devices, sent_to_all(): return lax.all_to_all(copies, axis, split_axis=0, concat_axis=0, tiled=True)  29.2 us
    another operation x1, loops' own time, per_device(): lax.scan(advance, carry, (key_blocks, value_blocks, jnp.arange(blocks, dt...  18.9 us
    dynamic_slice x32, local copies, waits for them, and re-layouts, per_device(): lax.scan(advance, carry, (key_blocks, value_blocks, jnp.arange(blocks, dt...  17.8 us
  transfers between devices with their start and end apart: 6, of which 6 were waited for; matrix products, arithmetic and copies ran while one was open for 5% of the time, Pallas kernels for 0%

commit v1 on v0

--- a/solution.py
+++ b/solution.py
@@ -1,9 +1,270 @@
-import math
-
 import jax
 import jax.numpy as jnp
 from jax import lax
+from jax.experimental import pallas as pl
+from jax.experimental.pallas import tpu as pltpu
 from jax.sharding import PartitionSpec as P
+
+
+MESH = pl.DeviceIdType.MESH
+LOG2E = 1.4426950408889634
+NEG = -1e30
+
+
+def place(half, chip_z, chip_y):
+    total = lax.rem(chip_y + chip_z, 4)
+    row = chip_y + half * (chip_z - chip_y)
+    return row * 4 + total
+
+
+def chip_at(half, position):
+    row = position // 4
+    other = lax.rem(lax.rem(position, 4) + 4 - row, 4)
+    chip_y = row + half * (other - row)
+    chip_z = other + half * (row - other)
+    return chip_z * 4 + chip_y
+
+
+def attend_kernel(
+    own_ref, even_ref, odd_ref, lam_ref, gain_ref,
+    att_ref, lse_ref,
+    kv, odd_in, queries, tops, totals, summed,
+    load_sem, odd_send, odd_recv, ring_send, ring_recv, twin_send, twin_recv,
+):
+    me = lax.axis_index("sp")
+    core = lax.rem(me, 2)
+    chip = me // 2
+    chip_z, chip_y = chip // 4, lax.rem(chip, 4)
+    twin = me + 1 - 2 * core
+    partner = 31 - me
+
+    def origin(half, direction, step):
+        here = place(half, chip_z, chip_y)
+        there = lax.rem(here + 16 - step + 2 * step * direction, 16)
+        return chip_at(half, there)
+
+    def onward(half, direction):
+        here = place(half, chip_z, chip_y)
+        there = lax.rem(here + 17 - 2 * direction, 16)
+        return chip_at(half, there) * 2 + core
+
+    def ring_copy(ring, step, sub):
+        half, direction = ring // 2, ring % 2
+        source = origin(half, direction, step - 1) * 2 + core
+        piece = kv.at[2 * source + half, sub]
+        return pltpu.make_async_remote_copy(
+            src_ref=piece, dst_ref=piece,
+            send_sem=ring_send.at[ring, step - 1, sub],
+            recv_sem=ring_recv.at[ring, step - 1, sub],
+            device_id={"sp": onward(half, direction)}, device_id_type=MESH,
+        )
+
+    def ring_arrival(ring, step, sub):
+        half, direction = ring // 2, ring % 2
+        source = origin(half, direction, step) * 2 + core
+        piece = kv.at[2 * source + half, sub]
+        return pltpu.make_async_remote_copy(
+            src_ref=piece, dst_ref=piece,
+            send_sem=ring_send.at[ring, step - 1, sub],
+            recv_sem=ring_recv.at[ring, step - 1, sub],
+            device_id={"sp": onward(half, direction)}, device_id_type=MESH,
+        )
+
+    def twin_copy(ring, step, sender):
+        half, direction = ring // 2, ring % 2
+        source = origin(half, direction, step) * 2 + sender
+        piece = kv.at[2 * source + half]
+        return pltpu.make_async_remote_copy(
+            src_ref=piece, dst_ref=piece,
+            send_sem=twin_send.at[ring, step],
+            recv_sem=twin_recv.at[ring, step],
+            device_id={"sp": twin}, device_id_type=MESH,
+        )
+
+    loads = []
+    for half in range(2):
+        loads.append(
+            pltpu.make_async_copy(own_ref.at[half], kv.at[2 * me + half], load_sem.at[half])
+        )
+        loads[-1].start()
+
+    barrier = pltpu.get_barrier_semaphore()
+    for ring in range(4):
+        pl.semaphore_signal(
+            barrier, inc=1, device_id={"sp": onward(ring // 2, ring % 2)}, device_id_type=MESH
+        )
+    pl.semaphore_signal(barrier, inc=1, device_id={"sp": twin}, device_id_type=MESH)
+    pl.semaphore_signal(barrier, inc=1, device_id={"sp": partner}, device_id_type=MESH)
+
+    for chunk in range(2):
+        for head in range(2):
+            tops[2 * chunk + head] = jnp.full((1, 512), NEG, jnp.float32)
+            totals[2 * chunk + head] = jnp.zeros((1, 512), jnp.float32)
+            summed[2 * chunk + head] = jnp.zeros((128, 512), jnp.float32)
+
+    def spread(chunk, head, block):
+        rows = lax.broadcasted_iota(jnp.int32, (128, 256), 0)
+        zero = jnp.zeros((128, 256), jnp.bfloat16)
+        queries[2 * chunk + head, :, 0:256] = jnp.where(rows < 64, block, zero)
+        queries[2 * chunk + head, :, 256:512] = jnp.where(rows < 64, zero, block)
+
+    for copy in loads:
+        copy.wait()
+    pl.semaphore_wait(barrier, 6)
+
+    for sub in range(4):
+        for ring in range(4):
+            ring_copy(ring, 1, sub).start()
+    odd_copy = pltpu.make_async_remote_copy(
+        src_ref=odd_ref, dst_ref=odd_in, send_sem=odd_send, recv_sem=odd_recv,
+        device_id={"sp": partner}, device_id_type=MESH,
+    )
+    odd_copy.start()
+    for half in range(2):
+        twin_copy(2 * half, 0, core).start()
+
+    for head in range(2):
+        spread(0, head, even_ref[head])
+    odd_copy.wait_recv()
+    for head in range(2):
+        spread(1, head, odd_in[head])
+
+    def advance(chunk, block, masked):
+        for head in range(2):
+            lanes = slice(128 * head, 128 * head + 128)
+            state = 2 * chunk + head
+            keys = jnp.concatenate([kv[block, 0, :, lanes], kv[block, 1, :, lanes]], axis=0)
+            scores = jnp.dot(keys, queries[state], preferred_element_type=jnp.float32)
+            if masked:
+                key_pos = lax.broadcasted_iota(jnp.int32, (256, 512), 0)
+                query_pos = lax.broadcasted_iota(jnp.int32, (256, 512), 1) & 255
+                scores = jnp.where(key_pos <= query_pos, scores, NEG)
+            before = tops[state]
+            top = jnp.maximum(before, jnp.max(scores, axis=0, keepdims=True))
+            weights = jnp.exp2(scores - top)
+            factor = jnp.exp2(before - top)
+            totals[state] = totals[state] * factor + jnp.sum(weights, axis=0, keepdims=True)
+            added = jnp.dot(
+                kv[block, 2 + head], weights.astype(jnp.bfloat16),
+                preferred_element_type=jnp.float32,
+            )
+            summed[state] = summed[state] * factor + added
+            tops[state] = top
+
+    def consider(chunk, block):
+        last = 2 * me + chunk * (63 - 4 * me)
+
+        @pl.when(block < last)
+        def _():
+            advance(chunk, block, False)
+
+        @pl.when(block == last)
+        def _():
+            advance(chunk, block, True)
+
+    def work(ring, step):
+        half, direction = ring // 2, ring % 2
+        source = origin(half, direction, step) * 2
+
+        def item(j, _):
+            turn, chunk = j // 2, lax.rem(j, 2)
+            sender = core + turn * (1 - 2 * core)
+
+            @pl.when(j == 2)
+            def _():
+                twin_copy(ring, step, 1 - core).wait_recv()
+
+            consider(chunk, 2 * (source + sender) + half)
+            return 0
+
+        lax.fori_loop(0, 4, item, 0)
+
+    def turn(t, _):
+        step, sub = t // 4 + 1, lax.rem(t, 4)
+        for ring in range(4):
+            ring_arrival(ring, step, sub).wait_recv()
+
+            @pl.when((step < 7) | (sub // 2 == ring % 2))
+            def _():
+                ring_copy(ring, step + 1, sub).start()
+
+        @pl.when(sub == 3)
+        def _():
+            for ring in range(4):
+                twin_copy(ring, step, core).start()
+
+        @pl.when((step > 1) | (lax.rem(sub, 2) == 0))
+        def _():
+            work(sub, step - 1)
+
+        return 0
+
+    lax.fori_loop(0, 28, turn, 0)
+
+    for half in range(2):
+        for sub in range(4):
+            ring_arrival(2 * half + sub // 2, 8, sub).wait_recv()
+        twin_copy(2 * half, 8, core).start()
+    lax.fori_loop(0, 4, lambda r, _: (work(r, 7), 0)[1], 0)
+    lax.fori_loop(0, 2, lambda h, _: (work(2 * h, 8), 0)[1], 0)
+
+    for chunk in range(2):
+        for head in range(2):
+            state = 2 * chunk + head
+            share = summed[state] / totals[state]
+            out = share[:, 0:256] - lam_ref[head] * share[:, 256:512]
+            power = jnp.mean(out * out, axis=0, keepdims=True)
+            out = out * lax.rsqrt(power + 1e-06) * gain_ref[...]
+            att_ref[chunk, :, 128 * head : 128 * head + 128] = out.T.astype(jnp.bfloat16)
+            lse_ref[chunk, head] = (tops[state] + jnp.log2(totals[state])) * (1.0 / LOG2E)
+
+    odd_copy.wait_send()
+    for half in range(2):
+        twin_copy(2 * half, 0, core).wait_send()
+        twin_copy(2 * half, 8, core).wait_send()
+
+    def drain(step, _):
+        for ring in range(4):
+            twin_copy(ring, step, core).wait_send()
+            for sub in range(4):
+                ring_copy(ring, step, sub).wait_send()
+        return 0
+
+    lax.fori_loop(1, 8, drain, 0)
+    for half in range(2):
+        for sub in range(4):
+            ring_copy(2 * half + sub // 2, 8, sub).wait_send()
+
+
+def attend(own, even, odd, lam, gain):
+    vmem = pl.BlockSpec(memory_space=pltpu.VMEM)
+    return pl.pallas_call(
+        attend_kernel,
+        out_shape=(
+            jax.ShapeDtypeStruct((2, 256, 256), jnp.bfloat16),
+            jax.ShapeDtypeStruct((2, 2, 1, 512), jnp.float32),
+        ),
+        in_specs=[pl.BlockSpec(memory_space=pl.ANY), vmem, vmem, vmem, vmem],
+        out_specs=(vmem, vmem),
+        scratch_shapes=[
+            pltpu.VMEM((64, 4, 128, 256), jnp.bfloat16),
+            pltpu.VMEM((2, 128, 256), jnp.bfloat16),
+            pltpu.VMEM((4, 128, 512), jnp.bfloat16),
+            pltpu.VMEM((4, 1, 512), jnp.float32),
+            pltpu.VMEM((4, 1, 512), jnp.float32),
+            pltpu.VMEM((4, 128, 512), jnp.float32),
+            pltpu.SemaphoreType.DMA((2,)),
+            pltpu.SemaphoreType.DMA,
+            pltpu.SemaphoreType.DMA,
+            pltpu.SemaphoreType.DMA((4, 8, 4)),
+            pltpu.SemaphoreType.DMA((4, 8, 4)),
+            pltpu.SemaphoreType.DMA((4, 9)),
+            pltpu.SemaphoreType.DMA((4, 9)),
+        ],
+        compiler_params=pltpu.CompilerParams(
+            collective_id=0, has_side_effects=True, vmem_limit_bytes=40 * 1024 * 1024
+        ),
+    )(own, even, odd, lam, gain)
 
 
 def joined_along(tiles, dim):
@@ -53,11 +314,11 @@
     )
 
 
-def prepare(raw, qk_gain, positions):
+def prepare(raw, qk_gain, positions, factor=1.0):
     values = raw.astype(jnp.float32)
     values = values * lax.rsqrt(jnp.mean(values * values, axis=-1, keepdims=True) + 1e-06)
     values = values * qk_gain[None, None, :, :]
-    return rotate(values, positions).astype(jnp.bfloat16)
+    return (rotate(values, positions) * factor).astype(jnp.bfloat16)
 
 
 def per_device(
@@ -110,71 +371,19 @@
     offset = lax.axis_index("sp") * tok_rows
     query_pos = offset + jnp.arange(tok_rows, dtype=jnp.int32)
     float_pos = query_pos.astype(jnp.float32)
-    rq = jnp.transpose(prepare(queries, qk_gain, float_pos), (1, 2, 0, 3))
-    rk = prepare(keys, qk_gain, float_pos)
-    scale = head_size ** (-0.5)
-    last_query = offset + tok_rows - 1
-    initial = (
-        jnp.full((heads_here, 2, tok_rows), -1e30, jnp.float32),
-        jnp.zeros((heads_here, 2, tok_rows), jnp.float32),
-        jnp.zeros((heads_here, 2, tok_rows, value_size), jnp.float32),
-    )
-    carry = initial
-    key_piece = lax.all_gather(rk, "sp", axis=0, tiled=True)
-    value_piece = lax.all_gather(values, "sp", axis=0, tiled=True)
-    count = key_piece.shape[0]
-    block = math.gcd(count, 512)
-    blocks = count // block
-    key_blocks = key_piece.reshape(blocks, block, heads_here, 2, head_size)
-    value_blocks = value_piece.reshape(blocks, block, heads_here, value_size)
-
-    def advance(state, item):
-        key_block, value_block, number = item
-        key_start = number * block
-
-        def compute(inner):
-            running, totals, summed = inner
-            scores = (
-                jnp.einsum("hmqd,khmd->hmqk", rq, key_block, preferred_element_type=jnp.float32)
-                * scale
-            )
-            key_pos = key_start + jnp.arange(block, dtype=jnp.int32)
-            allowed = key_pos[None, :] <= query_pos[:, None]
-            scores = jnp.where(allowed[None, None], scores, -1e30)
-            newtop = jnp.maximum(running, jnp.max(scores, axis=-1))
-            probs = jnp.where(allowed[None, None], jnp.exp(scores - newtop[..., None]), 0.0)
-            factor = jnp.exp(running - newtop)
-            totals = totals * factor + jnp.sum(probs, axis=-1)
-            added = jnp.einsum(
-                "hmqk,khd->hmqd",
-                probs.astype(jnp.bfloat16),
-                value_block,
-                preferred_element_type=jnp.float32,
-            )
-            return (newtop, totals, summed * factor[..., None] + added)
-
-        def keep(inner):
-            return inner
-
-        return (lax.cond(key_start <= last_query, compute, keep, state), None)
-
-    carry, unused = lax.scan(
-        advance, carry, (key_blocks, value_blocks, jnp.arange(blocks, dtype=jnp.int32))
-    )
-    running, totals, summed = carry
-    heads_out = (
-        summed[:, 0] / totals[:, 0, :, None]
-        - mix_lambda[:, None, None] * summed[:, 1] / totals[:, 1, :, None]
-    )
-    heads_out = (
-        heads_out
-        * lax.rsqrt(jnp.mean(heads_out * heads_out, axis=-1, keepdims=True) + 1e-06)
-        * head_gain
-    )
-    attended = jnp.transpose(heads_out.astype(jnp.bfloat16), (1, 0, 2)).reshape(
-        tok_rows, heads_here * value_size
-    )
-    log_totals = jnp.transpose(running + jnp.log(totals), (1, 0, 2))
+    scale = head_size ** (-0.5) * LOG2E
+    rq = prepare(queries, qk_gain, float_pos, scale).reshape(2, 256, heads_here, 2 * head_size)
+    rq = jnp.transpose(rq, (0, 2, 3, 1))
+    rk = prepare(keys, qk_gain, float_pos).reshape(2, 2, 128, heads_here * 2 * head_size)
+    flipped = jnp.transpose(values.reshape(2, 256, heads_here, value_size), (0, 2, 3, 1))
+    own = jnp.concatenate([rk, flipped], axis=1)
+    att, lse = attend(own, rq[0], rq[1], mix_lambda[:, None, None], head_gain[:, None])
+    count = lax.axis_size("sp")
+    swap = [(i, count - 1 - i) for i in range(count)]
+    attended = jnp.concatenate([att[0], lax.ppermute(att[1], "sp", swap)], axis=0)
+    logs = jnp.stack([lse[0], lax.ppermute(lse[1], "sp", swap)], axis=0)
+    logs = logs.reshape(2, heads_here, 2, 256)
+    log_totals = jnp.transpose(logs, (2, 1, 0, 3)).reshape(2, heads_here, tok_rows)
     gated = (glu_a.astype(jnp.float32) * jax.nn.sigmoid(glu_g.astype(jnp.float32))).astype(
         jnp.bfloat16
     )

time: 419 us -> 179 us (0.43)
  the two profiles are of different devices: /device:TPU:121 before, /device:TPU:16 now
where the time goes in v1:
time: 179 us; the launch traced here: 178 us
  Pallas kernels  95.3 us (53%)
  waiting for transfers between devices  41.2 us (23%)
  starting transfers between devices  14.4 us (8%)
  matrix products  12.8 us (7%)
  local copies, waits for them, and re-layouts  8.57 us (5%)
  other arithmetic  4.58 us (3%)
    pallas_call x1, Pallas kernels, attend(): pl.pallas_call(attend_kernel, out_shape=(jax.ShapeDtypeStruct((2, 256, 25...  95.3 us
    all_to_all x2, waiting for transfers between devices, sent_to_all(): return lax.all_to_all(copies, axis, split_axis=0, concat_axis=0, tiled=True)  30.3 us
    all_to_all x2, starting transfers between devices, sent_to_all(): return lax.all_to_all(copies, axis, split_axis=0, concat_axis=0, tiled=True)  7.68 us
    dot_general x5, matrix products, project(): jnp.dot(normed, matrix, preferred_element_type=jnp.float32)  7.3 us
    dot_general x1, matrix products, per_device(): jnp.einsum('rtcj,ctjd->rd', arranged, weight_view, preferred_element_type...  5.46 us
    ppermute x1, waiting for transfers between devices, per_device(): logs = jnp.stack([lse[0], lax.ppermute(lse[1], 'sp', swap)], axis=0)  5.11 us
    all_to_all x1, starting transfers between devices, per_device(): lax.all_to_all(merged, 'tp', split_axis=0, concat_axis=1, tiled=True)  4.47 us
  transfers between devices with their start and end apart: 6, of which 5 were waited for; matrix products, arithmetic and copies ran while one was open for 1% of the time, Pallas kernels for 54%

profile of v1, /device:TPU:16, one launch (start us, length us, event | category | flops | bytes accessed | tf_op | source)
XLA Modules:
  0.0 178.1 jit_solution(10595363389964034308)
XLA Ops:
  0.6 0.0 copy-start
  0.6 2.7 %broadcast_in_dim.8 = bf16[4,128,2048]{2,1,0:T(8,128)(2,1)} broadcast(bf16[128,2048]{1,0:T(8,128)(2,1)} %param.14), dimensions={1,2} | broadcast | bytes 2621440 | tf_op jit(solution)/shard_map/broadcast_in_dim | solution.py:277
  3.4 4.4 %all-to-all-start = ((bf16[4,128,2048]{2,1,0:T(8,128)(2,1)}), bf16[4,128,2048]{2,1,0:T(8,128)(2,1)S(1)}, u32[]{:S(2)}, u32[]{:S(2)}) async-start(bf16[4,128,2048]{2,1,0:T(8,128)(2,1)} %broadcast_in_dim.8), calls=%async_computation | async-start | bytes 4194304 | tf_op jit(solution)/shard_map/all_to_all | solution.py:278
  7.8 0.1 copy.41.gain_ref
  7.9 0.1 copy.40.lam_ref
  8.1 0.7 fusion.49
  8.7 0.3 multiply_cosine_fusion
  9.0 25.1 %all-to-all-done = bf16[4,128,2048]{2,1,0:T(8,128)(2,1)S(1)} async-done(((bf16[4,128,2048]{2,1,0:T(8,128)(2,1)}), bf16[4,128,2048]{2,1,0:T(8,128)(2,1)S(1)}, u32[]{:S(2)}, u32[]{:S(2)}) %all-to-all-start) | async-done | bytes 2097184 | tf_op jit(solution)/shard_map/all_to_all | solution.py:278
  34.1 0.5 multiply_reduce_fusion
  34.6 0.5 fusion.1
  35.2 0.0 copy-start.23
  35.2 0.8 fusion.13
  36.0 1.2 copy-done.23
  37.2 0.8 fusion.11
  38.0 0.2 fusion.14
  38.2 0.1 multiply_subtract_fusion
  38.3 0.0 copy-start.24
  38.4 0.1 convert_element_type.90
  38.6 0.1 convert_element_type.84
  38.6 0.2 copy.38
  38.8 0.8 copy-done.24
  39.6 2.3 %convolution_convert_fusion.3 = bf16[512,256]{1,0:T(8,128)(2,1)S(1)} fusion(bf16[512,2048]{1,0:T(8,128)(2,1)} %copy-done.1, bf16[2048,256]{1,0:T(8,128)(2,1)S(1)} %copy-done.24), kind=kOutput, calls=%fused_computation.9 | convolution fusion | flops 537001984 | bytes 3407872 | tf_op jit(solution)/shard_map/dot_general | solution.py:356
  41.9 0.1 reshape_reshape.3
  41.9 0.1 copy.37
  42.1 0.0 copy-start.25
  42.1 2.7 %fusion.10 = f32[512,256]{1,0:T(8,128)S(1)} fusion(bf16[512,2048]{1,0:T(8,128)(2,1)} %copy-done.1, bf16[2048,256]{1,0:T(8,128)(2,1)} %param.20), kind=kOutput, calls=%fused_computation.18 | convolution fusion | flops 537526272 | bytes 3670016 | tf_op jit(solution)/shard_map/dot_general | solution.py:356
  44.9 0.0 copy-done.25
  44.9 0.7 fusion.5
  45.6 0.0 copy-start.5
  45.8 2.1 %collective-permute-start.1 = (bf16[30,256]{1,0:T(8,128)(2,1)S(1)}, bf16[30,256]{1,0:T(8,128)(2,1)S(1)}, u32[]{:S(2)}, u32[]{:S(2)}) collective-permute-start(bf16[30,256]{1,0:T(8,128)(2,1)S(1)} %slice.306), channel_id=1, source_target_pairs={{0,4},{4,8},{8,12},{12,16},{16,20},{20,24},{24,28},{28,32},{32,36}... | collective-permute-start | bytes 46088 | tf_op jit(solution)/shard_map/ppermute | solution.py:288
  47.9 0.1 pad_maximum_fusion.own_ref
  47.9 95.3 %shard_map.149 = (bf16[2,256,256]{2,1,0:T(8,128)(2,1)S(1)}, f32[2,2,1,512]{3,2,1,0:T(1,128)S(1)}) custom-call(bf16[2,4,128,256]{3,2,1,0:T(8,128)(2,1)S(1)} %pad_maximum_fusion.own_ref, bf16[2,128,256]{2,1,0:T(8,128)(2,1)S(1)} %get-tuple-element.16.even_ref, bf16[2,128,256]{2,1,0:T(8,128)(2,1)S(1)} %get-tuple-element.15.odd_ref, ...), custom_call_target="tpu_custom_call" | custom-call | tf_op jit(solution)/shard_map/pallas_call | solution.py:241
  143.3 0.1 maximum_convert_fusion
  143.5 0.0 copy-start.20
  143.5 2.4 %fusion.47 = (f32[512]{0:T(512)S(1)}, f32[512]{0:T(512)S(1)}, f32[512,256]{1,0:T(8,128)S(1)}) fusion(f32[542,256]{1,0:T(8,128)S(1)} %maximum_convert_fusion, f32[256]{0:T(256)S(1)} %bitcast.110, f32[256]{0:T(256)S(1)} %bitcast.111, f32[256]{0:T(256)S(1)} %bitcast.113, f32[256]{0:T(256)S(1)} %bitcast.114, f32[256]{0:T(256)S(1)} %bitcast.115, ...), kind=kLoop, calls=%fused_computation.119 | loop fusion | flops 8387584 | bytes 16813056 | tf_op jit(solution)/shard_map/reduce_sum | solution.py:396
  145.9 0.6 broadcast_in_dim.11
  146.5 3.3 %all-to-all-start.1 = ((f32[4,1,1024]{2,1,0:T(1,128)}), f32[4,1,1024]{2,1,0:T(1,128)S(1)}, u32[]{:S(2)}, u32[]{:S(2)}) async-start(f32[4,1,1024]{2,1,0:T(1,128)} %broadcast_in_dim.11), calls=%async_computation.1 | async-start | bytes 32768 | tf_op jit(solution)/shard_map/all_to_all | solution.py:278
  149.8 0.1 collective-permute-start
  149.9 5.2 %all-to-all-done.1 = f32[4,1,1024]{2,1,0:T(1,128)S(1)} async-done(((f32[4,1,1024]{2,1,0:T(1,128)}), f32[4,1,1024]{2,1,0:T(1,128)S(1)}, u32[]{:S(2)}, u32[]{:S(2)}) %all-to-all-start.1) | async-done | bytes 16416 | tf_op jit(solution)/shard_map/all_to_all | solution.py:278
  155.2 0.3 multiply_convert_fusion
  155.4 2.3 %collective-permute-done = bf16[256,256]{1,0:T(8,128)(2,1)S(1)} collective-permute-done((bf16[256,256]{1,0:T(8,128)(2,1)S(1)}, bf16[256,256]{1,0:T(8,128)(2,1)S(1)}, u32[]{:S(2)}, u32[]{:S(2)}) %collective-permute-start) | collective-permute-done | bytes 131104 | tf_op jit(solution)/shard_map/ppermute | solution.py:383
  157.8 1.0 copy.43
  158.8 4.5 %all-to-all-start.2 = ((bf16[4,128,512]{1,2,0:T(8,128)(2,1)}), bf16[4,128,512]{1,2,0:T(8,128)(2,1)S(1)}, u32[]{:S(2)}, u32[]{:S(2)}) async-start(bf16[4,128,512]{1,2,0:T(8,128)(2,1)} %copy.43), calls=%async_computation.2 | async-start | bytes 1048576 | tf_op jit(solution)/shard_map/all_to_all | solution.py:408
  163.3 0.1 collective-permute-start.2
  163.4 5.1 %collective-permute-done.2 = f32[2,1,512]{2,1,0:T(1,128)S(1)} collective-permute-done((f32[2,1,512]{2,1,0:T(1,128)S(1)}, f32[2,1,512]{2,1,0:T(1,128)S(1)}, u32[]{:S(2)}, u32[]{:S(2)}) %collective-permute-start.2) | collective-permute-done | bytes 4128 | tf_op jit(solution)/shard_map/ppermute | solution.py:384
  168.6 0.6 reshape.145
  169.2 3.5 %all-to-all-done.2 = bf16[4,128,512]{1,2,0:T(8,128)(2,1)S(1)} async-done(((bf16[4,128,512]{1,2,0:T(8,128)(2,1)}), bf16[4,128,512]{1,2,0:T(8,128)(2,1)S(1)}, u32[]{:S(2)}, u32[]{:S(2)}) %all-to-all-start.2) | async-done | bytes 524320 | tf_op jit(solution)/shard_map/all_to_all | solution.py:408
  172.7 5.5 %fusion.2 = bf16[128,2048]{1,0:T(8,128)(2,1)} fusion(bf16[2,4,256,2048]{3,2,1,0:T(8,128)(2,1)} %bitcast.95, bf16[128,4,2,256]{0,3,2,1:T(8,128)(2,1)S(1)} %bitcast.96), kind=kOutput, calls=%fused_computation.5 | convolution fusion | flops 1074003968 | bytes 9437184 | tf_op jit(solution)/shard_map/rtcj,ctjd->rd/dot_general | solution.py:410
  (67 shorter events, 0.5 us)
Async XLA Ops:
  0.6 34.6 %copy-start = (bf16[2048,256]{1,0:T(8,128)(2,1)S(1)}, bf16[2048,256]{1,0:T(8,128)(2,1)}, u32[]{:S(2)}) copy-start(bf16[2048,256]{1,0:T(8,128)(2,1)} %param.16) | copy-start | bytes 3145732
  3.4 4.4 %copy-start.22 = (f32[128]{0:T(128)S(1)}, f32[128]{0:T(128)}, u32[]{:S(2)}) copy-start(f32[128]{0:T(128)} %param.23) | copy-start | bytes 1540
  3.4 4.5 %copy-start.26 = (f32[2]{0:T(128)S(1)}, f32[2]{0:T(128)}, u32[]{:S(2)}) copy-start(f32[2]{0:T(128)} %param.22) | copy-start | bytes 28
  3.4 4.7 %copy-start.3 = (f32[31,256]{1,0:T(8,128)S(1)}, f32[31,256]{1,0:T(8,128)}, u32[]{:S(2)}) copy-start(f32[31,256]{1,0:T(8,128)} %param.24) | copy-start | bytes 95236
  3.4 30.8 %all-to-all-start = ((bf16[4,128,2048]{2,1,0:T(8,128)(2,1)}), bf16[4,128,2048]{2,1,0:T(8,128)(2,1)S(1)}, u32[]{:S(2)}, u32[]{:S(2)}) async-start(bf16[4,128,2048]{2,1,0:T(8,128)(2,1)} %broadcast_in_dim.8), calls=%async_computation | async-start | bytes 4194304 | tf_op jit(solution)/shard_map/all_to_all | solution.py:278
  7.8 26.8 %copy-start.4 = (f32[2048]{0:T(1024)S(1)}, f32[2048]{0:T(1024)}, u32[]{:S(2)}) copy-start(f32[2048]{0:T(1024)} %param.15) | copy-start | bytes 24580
  35.2 2.8 %copy-start.1 = (bf16[512,2048]{1,0:T(8,128)(2,1)}, bf16[512,2048]{1,0:T(8,128)(2,1)S(1)}, u32[]{:S(2)}) copy-start(bf16[512,2048]{1,0:T(8,128)(2,1)S(1)} %fusion.1) | copy-start | bytes 6291460
  35.2 2.0 %copy-start.23 = (bf16[2048,256]{1,0:T(8,128)(2,1)S(1)}, bf16[2048,256]{1,0:T(8,128)(2,1)}, u32[]{:S(2)}) copy-start(bf16[2048,256]{1,0:T(8,128)(2,1)} %param.17) | copy-start | bytes 3145732
  37.2 0.8 copy-start.21
  38.3 1.2 copy-start.24
  42.1 2.8 %copy-start.2 = (bf16[512,2048]{1,0:T(8,128)(2,1)S(1)}, bf16[512,2048]{1,0:T(8,128)(2,1)}, u32[]{:S(2)}) copy-start(bf16[512,2048]{1,0:T(8,128)(2,1)} %copy-done.1) | copy-start | bytes 6291460
  42.1 2.8 %copy-start.25 = (bf16[2048,256]{1,0:T(8,128)(2,1)S(1)}, bf16[2048,256]{1,0:T(8,128)(2,1)}, u32[]{:S(2)}) copy-start(bf16[2048,256]{1,0:T(8,128)(2,1)} %param.19) | copy-start | bytes 3145732
  45.6 97.7 %copy-start.5 = (f32[1,256]{1,0:T(1,128)S(1)}, f32[1,256]{1,0:T(1,128)}, u32[]{:S(2)}) copy-start(f32[1,256]{1,0:T(1,128)} %get-tuple-element.24) | copy-start | bytes 3076
  45.6 97.7 %copy-start.6 = (f32[1,256]{1,0:T(1,128)S(1)}, f32[1,256]{1,0:T(1,128)}, u32[]{:S(2)}) copy-start(f32[1,256]{1,0:T(1,128)} %get-tuple-element.25) | copy-start | bytes 3076
  45.6 97.7 %copy-start.7 = (f32[1,256]{1,0:T(1,128)S(1)}, f32[1,256]{1,0:T(1,128)}, u32[]{:S(2)}) copy-start(f32[1,256]{1,0:T(1,128)} %get-tuple-element.26) | copy-start | bytes 3076
  45.6 97.7 %copy-start.8 = (f32[1,256]{1,0:T(1,128)S(1)}, f32[1,256]{1,0:T(1,128)}, u32[]{:S(2)}) copy-start(f32[1,256]{1,0:T(1,128)} %get-tuple-element.27) | copy-start | bytes 3076
  45.6 97.7 %copy-start.9 = (f32[1,256]{1,0:T(1,128)S(1)}, f32[1,256]{1,0:T(1,128)}, u32[]{:S(2)}) copy-start(f32[1,256]{1,0:T(1,128)} %get-tuple-element.28) | copy-start | bytes 3076
  45.7 97.7 %copy-start.10 = (f32[1,256]{1,0:T(1,128)S(1)}, f32[1,256]{1,0:T(1,128)}, u32[]{:S(2)}) copy-start(f32[1,256]{1,0:T(1,128)} %get-tuple-element.29) | copy-start | bytes 3076
  45.7 97.7 %copy-start.11 = (f32[1,256]{1,0:T(1,128)S(1)}, f32[1,256]{1,0:T(1,128)}, u32[]{:S(2)}) copy-start(f32[1,256]{1,0:T(1,128)} %get-tuple-element.30) | copy-start | bytes 3076
  45.7 97.7 %copy-start.12 = (f32[1,256]{1,0:T(1,128)S(1)}, f32[1,256]{1,0:T(1,128)}, u32[]{:S(2)}) copy-start(f32[1,256]{1,0:T(1,128)} %get-tuple-element.31) | copy-start | bytes 3076
  45.7 97.7 %copy-start.13 = (f32[1,256]{1,0:T(1,128)S(1)}, f32[1,256]{1,0:T(1,128)}, u32[]{:S(2)}) copy-start(f32[1,256]{1,0:T(1,128)} %get-tuple-element.32) | copy-start | bytes 3076
  45.7 97.7 %copy-start.14 = (f32[1,256]{1,0:T(1,128)S(1)}, f32[1,256]{1,0:T(1,128)}, u32[]{:S(2)}) copy-start(f32[1,256]{1,0:T(1,128)} %get-tuple-element.33) | copy-start | bytes 3076
  45.7 97.7 %copy-start.15 = (f32[1,256]{1,0:T(1,128)S(1)}, f32[1,256]{1,0:T(1,128)}, u32[]{:S(2)}) copy-start(f32[1,256]{1,0:T(1,128)} %get-tuple-element.34) | copy-start | bytes 3076
  45.7 97.7 %copy-start.16 = (f32[1,256]{1,0:T(1,128)S(1)}, f32[1,256]{1,0:T(1,128)}, u32[]{:S(2)}) copy-start(f32[1,256]{1,0:T(1,128)} %get-tuple-element.35) | copy-start | bytes 3076
  45.7 97.7 %copy-start.17 = (f32[1,256]{1,0:T(1,128)S(1)}, f32[1,256]{1,0:T(1,128)}, u32[]{:S(2)}) copy-start(f32[1,256]{1,0:T(1,128)} %get-tuple-element.36) | copy-start | bytes 3076
  45.7 97.7 %copy-start.18 = (f32[1,256]{1,0:T(1,128)S(1)}, f32[1,256]{1,0:T(1,128)}, u32[]{:S(2)}) copy-start(f32[1,256]{1,0:T(1,128)} %get-tuple-element.37) | copy-start | bytes 3076
  45.8 97.5 %collective-permute-start.1 = (bf16[30,256]{1,0:T(8,128)(2,1)S(1)}, bf16[30,256]{1,0:T(8,128)(2,1)S(1)}, u32[]{:S(2)}, u32[]{:S(2)}) collective-permute-start(bf16[30,256]{1,0:T(8,128)(2,1)S(1)} %slice.306), channel_id=1, source_target_pairs={{0,4},{4,8},{8,12},{12,16},{16,20},{20,24},{24,28},{28,32},{32,36}... | collective-permute-start | bytes 46088 | tf_op jit(solution)/shard_map/ppermute | solution.py:288
  143.5 11.7 %copy-start.19 = (f32[256]{0:T(256)S(1)}, f32[256]{0:T(256)}, u32[]{:S(2)}) copy-start(f32[256]{0:T(256)} %param.26) | copy-start | bytes 3076
  143.5 11.7 %copy-start.20 = (f32[256]{0:T(256)S(1)}, f32[256]{0:T(256)}, u32[]{:S(2)}) copy-start(f32[256]{0:T(256)} %param.25) | copy-start | bytes 3076
  146.5 8.6 %all-to-all-start.1 = ((f32[4,1,1024]{2,1,0:T(1,128)}), f32[4,1,1024]{2,1,0:T(1,128)S(1)}, u32[]{:S(2)}, u32[]{:S(2)}) async-start(f32[4,1,1024]{2,1,0:T(1,128)} %broadcast_in_dim.11), calls=%async_computation.1 | async-start | bytes 32768 | tf_op jit(solution)/shard_map/all_to_all | solution.py:278
  149.8 7.9 %collective-permute-start = (bf16[256,256]{1,0:T(8,128)(2,1)S(1)}, bf16[256,256]{1,0:T(8,128)(2,1)S(1)}, u32[]{:S(2)}, u32[]{:S(2)}) collective-permute-start(bf16[256,256]{1,0:T(8,128)(2,1)S(1)} %get-tuple-element.14), channel_id=1, source_target_pairs={{0,124},{4,120},{8,116},{12,112},{16,108},{20,104},{24,100},{28,96... | collective-permute-start | bytes 393224 | tf_op jit(solution)/shard_map/ppermute | solution.py:383
  158.8 13.9 %all-to-all-start.2 = ((bf16[4,128,512]{1,2,0:T(8,128)(2,1)}), bf16[4,128,512]{1,2,0:T(8,128)(2,1)S(1)}, u32[]{:S(2)}, u32[]{:S(2)}) async-start(bf16[4,128,512]{1,2,0:T(8,128)(2,1)} %copy.43), calls=%async_computation.2 | async-start | bytes 1048576 | tf_op jit(solution)/shard_map/all_to_all | solution.py:408
  163.3 5.2 %collective-permute-start.2 = (f32[2,1,512]{2,1,0:T(1,128)S(1)}, f32[2,1,512]{2,1,0:T(1,128)S(1)}, u32[]{:S(2)}, u32[]{:S(2)}) collective-permute-start(f32[2,1,512]{2,1,0:T(1,128)S(1)} %get-tuple-element.51), channel_id=1, source_target_pairs={{0,124},{4,120},{8,116},{12,112},{16,108},{20,104},{24,100},{28,96... | collective-permute-start | bytes 12296 | tf_op jit(solution)/shard_map/ppermute | solution.py:384

commit v2 on v1

v2 whole, which is shorter than its diff:
```python
import jax
import jax.numpy as jnp
from jax import lax
from jax.experimental import pallas as pl
from jax.experimental.pallas import tpu as pltpu
from jax.sharding import PartitionSpec as P

MESH = pl.DeviceIdType.MESH
LOG2E = 1.4426950408889634
NEG = -1e30
SUBS = 4
SUB_ROWS = 512 // SUBS


def place(half, chip_z, chip_y):
    total = lax.rem(chip_y + chip_z, 4)
    row = chip_y + half * (chip_z - chip_y)
    return row * 4 + total


def chip_at(half, position):
    row = position // 4
    other = lax.rem(lax.rem(position, 4) + 4 - row, 4)
    chip_y = row + half * (other - row)
    chip_z = other + half * (row - other)
    return chip_z * 4 + chip_y


def attend_kernel(
    own_ref, query_ref, gated_ref, lam_ref, gain_ref, taps_ref, scale_ref, shift_ref, out_w_ref,
    mixed_ref, logs_ref,
    kv, odd_in, queries, tops, totals, summed,
    halo, shifted, convolved, sums, conv_out, conv_in, attended, attended_in, logs_in, out_w, mixing,
    load_sem, odd_send, odd_recv, ring_send, ring_recv, twin_send, twin_recv,
    weight_sem, halo_sem, sums_send, sums_recv, conv_send, conv_recv, att_send, att_recv, logs_sem,
):
    me = lax.axis_index("sp")
    group = lax.axis_index("tp")
    core = lax.rem(me, 2)
    chip = me // 2
    chip_z, chip_y = chip // 4, lax.rem(chip, 4)
    twin = me + 1 - 2 * core
    partner = 31 - me

    def origin(half, direction, step):
        here = place(half, chip_z, chip_y)
        there = lax.rem(here + 16 - step + 2 * step * direction, 16)
        return chip_at(half, there)

    def onward(half, direction):
        here = place(half, chip_z, chip_y)
        there = lax.rem(here + 17 - 2 * direction, 16)
        return chip_at(half, there) * 2 + core

    def ring_copy(ring, step, sub):
        half, direction = ring // 2, ring % 2
        source = origin(half, direction, step - 1) * 2 + core
        piece = kv.at[2 * source + half, pl.ds(sub * SUB_ROWS, SUB_ROWS)]
        return pltpu.make_async_remote_copy(
            src_ref=piece, dst_ref=piece,
            send_sem=ring_send.at[ring, step - 1, sub],
            recv_sem=ring_recv.at[ring, step - 1, sub],
            device_id={"sp": onward(half, direction)}, device_id_type=MESH,
        )

    def ring_arrival(ring, step, sub):
        half, direction = ring // 2, ring % 2
        source = origin(half, direction, step) * 2 + core
        piece = kv.at[2 * source + half, pl.ds(sub * SUB_ROWS, SUB_ROWS)]
        return pltpu.make_async_remote_copy(
            src_ref=piece, dst_ref=piece,
            send_sem=ring_send.at[ring, step - 1, sub],
            recv_sem=ring_recv.at[ring, step - 1, sub],
            device_id={"sp": onward(half, direction)}, device_id_type=MESH,
        )

    def twin_copy(ring, step, sender):
        half, direction = ring // 2, ring % 2
        source = origin(half, direction, step) * 2 + sender
        piece = kv.at[2 * source + half]
        return pltpu.make_async_remote_copy(
            src_ref=piece, dst_ref=piece,
            send_sem=twin_send.at[ring, step],
            recv_sem=twin_recv.at[ring, step],
            device_id={"sp": twin}, device_id_type=MESH,
        )

    loads = []
    for half in range(2):
        loads.append(
            pltpu.make_async_copy(own_ref.at[half], kv.at[2 * me + half], load_sem.at[half])
        )
        loads[-1].start()

    fetch = pltpu.make_async_copy(out_w_ref, out_w, weight_sem)
    fetch.start()

    barrier = pltpu.get_barrier_semaphore()
    for ring in range(4):
        pl.semaphore_signal(
            barrier, inc=1, device_id={"sp": onward(ring // 2, ring % 2)}, device_id_type=MESH
        )
    pl.semaphore_signal(barrier, inc=1, device_id={"sp": twin}, device_id_type=MESH)
    after, before_me = lax.rem(me + 1, 32), lax.rem(me + 31, 32)
    for place_on_line in (after, before_me):
        pl.semaphore_signal(barrier, inc=1, device_id={"sp": place_on_line}, device_id_type=MESH)
    for hop in range(4):
        peer = lax.rem(group + hop, 4)
        pl.semaphore_signal(
            barrier, inc=1, device_id={"sp": partner, "tp": peer}, device_id_type=MESH
        )
        if hop > 0:
            pl.semaphore_signal(barrier, inc=1, device_id={"tp": peer}, device_id_type=MESH)

    for chunk in range(2):
        for head in range(2):
            tops[2 * chunk + head] = jnp.full((1, 512), NEG, jnp.float32)
            totals[2 * chunk + head] = jnp.zeros((1, 512), jnp.float32)
            summed[2 * chunk + head] = jnp.zeros((128, 512), jnp.float32)

    def spread(chunk, head, block):
        rows = lax.broadcasted_iota(jnp.int32, (128, 256), 0)
        zero = jnp.zeros((128, 256), jnp.bfloat16)
        queries[2 * chunk + head, :, 0:256] = jnp.where(rows < 64, block, zero)
        queries[2 * chunk + head, :, 256:512] = jnp.where(rows < 64, zero, block)

    for copy in loads:
        copy.wait()
    pl.semaphore_wait(barrier, 14)

    for sub in range(SUBS):
        for ring in range(4):
            ring_copy(ring, 1, sub).start()
    odd_copy = pltpu.make_async_remote_copy(
        src_ref=query_ref.at[1], dst_ref=odd_in, send_sem=odd_send, recv_sem=odd_recv,
        device_id={"sp": partner}, device_id_type=MESH,
    )
    odd_copy.start()
    halo_copy = pltpu.make_async_remote_copy(
        src_ref=gated_ref.at[pl.ds(480, 32)], dst_ref=halo,
        send_sem=halo_sem.at[0], recv_sem=halo_sem.at[1],
        device_id={"sp": after}, device_id_type=MESH,
    )
    halo_copy.start()
    for half in range(2):
        twin_copy(2 * half, 0, core).start()

    for head in range(2):
        spread(0, head, query_ref[0, head])
    odd_copy.wait_recv()
    for head in range(2):
        spread(1, head, odd_in[head])

    def to_peers(source, target, send, recv, hop, rows=None):
        peer = lax.rem(group + hop, 4)
        piece = source if rows is None else source.at[pl.ds(pl.multiple_of(rows * peer, 16), rows)]
        return pltpu.make_async_remote_copy(
            src_ref=piece, dst_ref=target.at[4 - hop],
            send_sem=send.at[4 - hop], recv_sem=recv.at[4 - hop],
            device_id={"tp": peer}, device_id_type=MESH,
        )

    def sums_copy(hop):
        return to_peers(sums.at[0], sums, sums_send, sums_recv, hop)

    def conv_copy(hop):
        return to_peers(conv_out, conv_in, conv_send, conv_recv, hop, 128)

    halo_copy.wait_recv()
    first = jnp.where(me == 0, jnp.zeros((32, 256), jnp.float32), halo[...].astype(jnp.float32))
    shifted[0, 0:32, :] = first
    shifted[0, 32:544, :] = gated_ref[...].astype(jnp.float32)
    for shift in range(1, 8):
        shifted[shift, 0:536, :] = shifted[0, shift : shift + 536, :]

    def conv_tile(tile, _):
        base = tile * 32
        total = jnp.zeros((32, 256), jnp.float32)
        for tap in range(31):
            offset = tap + 2
            start = pl.multiple_of(base + offset // 8 * 8, 8)
            total = total + taps_ref[tap : tap + 1, :] * shifted[offset % 8, pl.ds(start, 32), :]
        convolved[pl.ds(pl.multiple_of(base, 32), 32), :] = total
        return 0

    lax.fori_loop(0, 16, conv_tile, 0)
    lanes = lax.broadcasted_iota(jnp.int32, (512, 128), 1)
    conv_now = convolved[...]
    plain = jnp.sum(conv_now, axis=1, keepdims=True)
    square = jnp.sum(conv_now * conv_now, axis=1, keepdims=True)
    both = jnp.where(lanes == 0, plain, jnp.where(lanes == 1, square, 0.0))
    sums[0] = both.T[0:8]

    def normalize():
        for hop in range(1, 4):
            sums_copy(hop).wait_recv()
        total = sums[0] + sums[1] + sums[2] + sums[3]
        padded = jnp.concatenate([total, jnp.zeros((120, 512), jnp.float32)], axis=0).T
        middle = padded[:, 0:1] / 1024.0
        spread_now = padded[:, 1:2] / 1024.0 - middle * middle
        value = (convolved[...] - middle) * lax.rsqrt(spread_now + 1e-05)
        value = value * scale_ref[...] + shift_ref[...]
        conv_out[...] = (value * jax.nn.sigmoid(value)).astype(jnp.bfloat16)

    def mix(pieces, top_row, start):
        order = [lax.rem(group + hop, 4) for hop in range(4)]

        def columns(n, _):
            span = pl.ds(pl.multiple_of(512 * n, 512), 512)
            total = jnp.zeros((128, 512), jnp.float32) if start is None else start[:, span]
            for hop in range(4):
                rows = pl.ds(pl.multiple_of(top_row + 256 * order[hop], 256), 256)
                total = total + jnp.dot(
                    pieces[hop], out_w[rows, span], preferred_element_type=jnp.float32
                )
            if start is None:
                mixing[:, span] = total
            else:
                mixed_ref[:, span] = total.astype(jnp.bfloat16)
            return 0

        lax.fori_loop(0, 4, columns, 0)

    def advance(chunk, blocks, masked):
        states = [2 * chunk + head for head in range(2)]
        before = [tops[state] for state in states]
        sums = [totals[state] for state in states]
        scores = []
        for head in range(2):
            lanes = slice(128 * head, 128 * head + 128)
            keys = jnp.concatenate([kv[block, 0:256, lanes] for block in blocks], axis=0)
            scores.append(
                jnp.dot(keys, queries[states[head]], preferred_element_type=jnp.float32)
            )
        if masked:
            rows = len(blocks) * 256
            key_pos = lax.broadcasted_iota(jnp.int32, (rows, 512), 0) + 256 * blocks[0]
            query_pos = lax.broadcasted_iota(jnp.int32, (rows, 512), 1) & 255
            last = 2 * me + chunk * (63 - 4 * me)
            allowed = key_pos <= query_pos + 256 * last
            scores = [jnp.where(allowed, part, NEG) for part in scores]
        after = []
        for head in range(2):
            top = jnp.maximum(before[head], jnp.max(scores[head], axis=0, keepdims=True))
            weights = jnp.exp2(scores[head] - top)
            factor = jnp.exp2(before[head] - top)
            total = sums[head] * factor + jnp.sum(weights, axis=0, keepdims=True)
            shares = kv_values(blocks, head)
            added = jnp.dot(
                shares, weights.astype(jnp.bfloat16), preferred_element_type=jnp.float32
            )
            after.append((top, total, factor, added))
        for head in range(2):
            top, total, factor, added = after[head]
            tops[states[head]] = top
            totals[states[head]] = total
            summed[states[head]] = summed[states[head]] * factor + added

    def kv_values(blocks, head):
        rows = slice(256 + 128 * head, 384 + 128 * head)
        return jnp.concatenate([kv[block, rows, :] for block in blocks], axis=1)

    def work(ring, step):
        half, direction = ring // 2, ring % 2
        low = 4 * origin(half, direction, step) + half
        twin_copy(ring, step, 1 - core).wait_recv()
        for chunk in range(2):
            last = 2 * me + chunk * (63 - 4 * me)

            @pl.when(low + 2 < last)
            def _():
                advance(chunk, [low, low + 2], False)

            @pl.when(low + 2 >= last)
            def _():
                def item(j, _):
                    @pl.when(low + 2 * j <= last)
                    def _():
                        advance(chunk, [low + 2 * j], True)

                    return 0

                lax.fori_loop(0, 2, item, 0)

    def turn(t, _):
        step, part = t // 4 + 1, lax.rem(t, 4)
        for piece in range(SUBS // 4):
            sub = part * (SUBS // 4) + piece
            for ring in range(4):
                ring_arrival(ring, step, sub).wait_recv()

                @pl.when((step < 7) | (sub // (SUBS // 2) == ring % 2))
                def _():
                    ring_copy(ring, step + 1, sub).start()

        @pl.when(part == 3)
        def _():
            for ring in range(4):
                twin_copy(ring, step, core).start()

        @pl.when(t == 0)
        def _():
            for hop in range(1, 4):
                sums_copy(hop).start()

        @pl.when(t == 4)
        def _():
            normalize()

        @pl.when(t == 6)
        def _():
            for hop in range(1, 4):
                conv_copy(hop).start()
            mine = pl.ds(pl.multiple_of(128 * group, 128), 128)
            conv_in[0] = conv_out[mine, :]

        @pl.when(t == 12)
        def _():
            fetch.wait()
            for hop in range(1, 4):
                conv_copy(hop).wait_recv()
            mix(conv_in, 1024, None)

        @pl.when((step > 1) | (lax.rem(part, 2) == 0))
        def _():
            work(part, step - 1)

        return 0

    lax.fori_loop(0, 28, turn, 0)

    for half in range(2):
        for sub in range(SUBS):
            ring_arrival(2 * half + sub // (SUBS // 2), 8, sub).wait_recv()
        twin_copy(2 * half, 8, core).start()
    lax.fori_loop(0, 4, lambda r, _: (work(r, 7), 0)[1], 0)
    lax.fori_loop(0, 2, lambda h, _: (work(2 * h, 8), 0)[1], 0)

    logs_copy = pltpu.make_async_remote_copy(
        src_ref=logs_in.at[1], dst_ref=logs_in.at[2],
        send_sem=logs_sem.at[0], recv_sem=logs_sem.at[1],
        device_id={"sp": partner}, device_id_type=MESH,
    )

    def att_copy(part, target_sp, slot):
        return pltpu.make_async_remote_copy(
            src_ref=attended.at[part // 2, pl.ds(128 * (part % 2), 128)],
            dst_ref=attended_in.at[slot],
            send_sem=att_send.at[part], recv_sem=att_recv.at[slot],
            device_id={"sp": target_sp, "tp": part}, device_id_type=MESH,
        )

    for chunk in (1, 0):
        for head in range(2):
            state = 2 * chunk + head
            share = summed[state] / totals[state]
            out = share[:, 0:256] - lam_ref[head] * share[:, 256:512]
            power = jnp.mean(out * out, axis=0, keepdims=True)
            out = out * lax.rsqrt(power + 1e-06) * gain_ref[...]
            attended[chunk, :, 128 * head : 128 * head + 128] = out.T.astype(jnp.bfloat16)
            logs_in[chunk, head] = (tops[state] + jnp.log2(totals[state])) * (1.0 / LOG2E)

    for part in (2, 3):
        att_copy(part, partner, lax.rem(group + 4 - part, 4)).start()
    for part in (0, 1):

        @pl.when(group != part)
        def _():
            att_copy(part, me, lax.rem(group + 4 - part, 4)).start()

        @pl.when(group == part)
        def _():
            attended_in[0] = attended[0, 128 * part : 128 * part + 128, :]

    logs_copy.start()
    for slot in range(4):

        @pl.when((group >= 2) | (slot > 0))
        def _():
            att_copy(0, partner, slot).wait_recv()

    mix(attended_in, 0, mixing)

    logs_copy.wait()
    for head in range(2):
        for half in range(2):
            columns = slice(256 * half, 256 * half + 256)
            logs_ref[half, head : head + 1, 0:256] = logs_in[0, head, :, columns]
            logs_ref[half, head : head + 1, 256:512] = logs_in[2, head, :, columns]

    for part in (2, 3):
        att_copy(part, partner, lax.rem(group + 4 - part, 4)).wait_send()
    for part in (0, 1):

        @pl.when(group != part)
        def _():
            att_copy(part, me, lax.rem(group + 4 - part, 4)).wait_send()

    halo_copy.wait_send()
    for hop in range(1, 4):
        sums_copy(hop).wait_send()
        conv_copy(hop).wait_send()
    odd_copy.wait_send()
    for half in range(2):
        twin_copy(2 * half, 0, core).wait_send()
        twin_copy(2 * half, 8, core).wait_send()

    def drain(step, _):
        for ring in range(4):
            twin_copy(ring, step, core).wait_send()
            for sub in range(SUBS):
                ring_copy(ring, step, sub).wait_send()
        return 0

    lax.fori_loop(1, 8, drain, 0)
    for half in range(2):
        for sub in range(SUBS):
            ring_copy(2 * half + sub // (SUBS // 2), 8, sub).wait_send()


def attend(own, queries, gated, lam, gain, taps, scale, shift, out_w):
    vmem = pl.BlockSpec(memory_space=pltpu.VMEM)
    hbm = pl.BlockSpec(memory_space=pl.ANY)
    dma = pltpu.SemaphoreType.DMA
    return pl.pallas_call(
        attend_kernel,
        out_shape=(
            jax.ShapeDtypeStruct((128, 2048), jnp.bfloat16),
            jax.ShapeDtypeStruct((2, 2, 512), jnp.float32),
        ),
        in_specs=[hbm] + [vmem] * 7 + [hbm],
        out_specs=(vmem, vmem),
        scratch_shapes=[
            pltpu.VMEM((64, 512, 256), jnp.bfloat16),
            pltpu.VMEM((2, 128, 256), jnp.bfloat16),
            pltpu.VMEM((4, 128, 512), jnp.bfloat16),
            pltpu.VMEM((4, 1, 512), jnp.float32),
            pltpu.VMEM((4, 1, 512), jnp.float32),
            pltpu.VMEM((4, 128, 512), jnp.float32),
            pltpu.VMEM((32, 256), jnp.bfloat16),
            pltpu.VMEM((8, 544, 256), jnp.float32),
            pltpu.VMEM((512, 256), jnp.float32),
            pltpu.VMEM((4, 8, 512), jnp.float32),
            pltpu.VMEM((512, 256), jnp.bfloat16),
            pltpu.VMEM((4, 128, 256), jnp.bfloat16),
            pltpu.VMEM((2, 256, 256), jnp.bfloat16),
            pltpu.VMEM((4, 128, 256), jnp.bfloat16),
            pltpu.VMEM((3, 2, 1, 512), jnp.float32),
            pltpu.VMEM((2048, 2048), jnp.bfloat16),
            pltpu.VMEM((128, 2048), jnp.float32),
            dma((2,)), dma, dma, dma((4, 8, SUBS)), dma((4, 8, SUBS)), dma((4, 9)), dma((4, 9)),
            dma, dma((2,)), dma((4,)), dma((4,)), dma((4,)), dma((4,)), dma((4,)), dma((4,)), dma((2,)),
        ],
        compiler_params=pltpu.CompilerParams(
            collective_id=0, has_side_effects=True, vmem_limit_bytes=48 * 1024 * 1024
        ),
    )(own, queries, gated, lam, gain, taps, scale, shift, out_w)


def project_kernel(
    tok_ref, wq_ref, wk_ref, wv_ref, wa_ref, wg_ref, gain_ref, qk_ref, trig_ref,
    own_ref, query_ref, gated_ref,
    rows, weights, load_sem, weight_sem, send_sem, recv_sem, far_send, far_recv,
):
    me = lax.axis_index("tp")
    right, left = lax.rem(me + 1, 4), lax.rem(me + 3, 4)
    far = lax.rem(me + 2, 4)

    load = pltpu.make_async_copy(tok_ref, rows.at[me], load_sem)
    load.start()
    fetches = []
    for n, ref in enumerate((wq_ref, wk_ref, wv_ref, wa_ref, wg_ref)):
        fetches.append(
            pltpu.make_async_copy(ref, weights.at[:, pl.ds(256 * n, 256)], weight_sem.at[n])
        )
        fetches[-1].start()

    barrier = pltpu.get_barrier_semaphore()
    for peer in (left, right):
        pl.semaphore_signal(barrier, inc=1, device_id={"tp": peer}, device_id_type=MESH)
    load.wait()
    pl.semaphore_wait(barrier, 2)

    def hand(block, direction, half, send, recv):
        piece = rows.at[block, pl.ds(64 * half, 64)]
        return pltpu.make_async_remote_copy(
            src_ref=piece, dst_ref=piece, send_sem=send, recv_sem=recv,
            device_id={"tp": right if direction == 0 else left}, device_id_type=MESH,
        )

    def near(direction, half, block):
        return hand(
            block, direction, half, send_sem.at[direction, half], recv_sem.at[direction, half]
        )

    def beyond(direction, block):
        return hand(block, direction, direction, far_send.at[direction], far_recv.at[direction])

    for turn in range(2):
        near(0, turn, me).start()
        near(1, 1 - turn, me).start()

    def project(block):
        inputs = rows[block].astype(jnp.float32)
        power = jnp.mean(inputs * inputs, axis=-1, keepdims=True)
        normed = (inputs * lax.rsqrt(power + 1e-06) * gain_ref[...]).astype(jnp.bfloat16)
        places = pl.ds(pl.multiple_of(128 * block, 128), 128)
        pair, side = block // 2, pl.ds(pl.multiple_of(128 * lax.rem(block, 2), 128), 128)
        cosine, sine = trig_ref[0, :, places], trig_ref[1, :, places]

        def product(n):
            return jnp.dot(
                normed, weights[:, 256 * n : 256 * n + 256], preferred_element_type=jnp.float32
            ).astype(jnp.bfloat16).astype(jnp.float32)

        def prepared(flat, which):
            parts = []
            for group in range(4):
                piece = flat[64 * group : 64 * group + 64]
                power = jnp.mean(piece * piece, axis=0, keepdims=True)
                gains = qk_ref[which, 64 * group : 64 * group + 64]
                piece = piece * lax.rsqrt(power + 1e-06) * gains
                first, second = piece[:32], piece[32:]
                parts.append(first * cosine - second * sine)
                parts.append(second * cosine + first * sine)
            return jnp.concatenate(parts, axis=0)

        turned = prepared(product(0).T, 0).astype(jnp.bfloat16)
        for head in range(2):
            query_ref[pair, head, :, side] = turned[128 * head : 128 * head + 128]
        own_ref[pair, side, :] = prepared(product(1).T, 1).T.astype(jnp.bfloat16)
        own_ref[pair, 256:512, side] = product(2).T.astype(jnp.bfloat16)
        gated = product(3) * jax.nn.sigmoid(product(4))
        gated_ref[places, :] = gated.astype(jnp.bfloat16)

    for fetch in fetches:
        fetch.wait()

    def turn(n, _):
        block = lax.rem(me + n + n // 2 - 2 * (n // 3), 4)

        @pl.when(n == 1)
        def _():
            near(0, 0, left).wait_recv()
            beyond(0, left).start()
            near(1, 1, right).wait_recv()
            beyond(1, right).start()
            near(1, 0, right).wait_recv()

        @pl.when(n == 2)
        def _():
            near(0, 1, left).wait_recv()

        @pl.when(n == 3)
        def _():
            beyond(0, far).wait_recv()
            beyond(1, far).wait_recv()

        project(block)
        return 0

    lax.fori_loop(0, 4, turn, 0)

    for direction in range(2):
        for half in range(2):
            near(direction, half, me).wait_send()
        beyond(direction, left if direction == 0 else right).wait_send()


def project_all(tokens, matrices, norm_gain, qk, trig):
    vmem = pl.BlockSpec(memory_space=pltpu.VMEM)
    hbm = pl.BlockSpec(memory_space=pl.ANY)
    return pl.pallas_call(
        project_kernel,
        out_shape=(
            jax.ShapeDtypeStruct((2, 512, 256), jnp.bfloat16),
            jax.ShapeDtypeStruct((2, 2, 128, 256), jnp.bfloat16),
            jax.ShapeDtypeStruct((512, 256), jnp.bfloat16),
        ),
        in_specs=[hbm] * 6 + [vmem] * 3,
        out_specs=(vmem, vmem, vmem),
        scratch_shapes=[
            pltpu.VMEM((4, 128, 2048), jnp.bfloat16),
            pltpu.VMEM((2048, 1280), jnp.bfloat16),
            pltpu.SemaphoreType.DMA,
            pltpu.SemaphoreType.DMA((5,)),
            pltpu.SemaphoreType.DMA((2, 2)),
            pltpu.SemaphoreType.DMA((2, 2)),
            pltpu.SemaphoreType.DMA((2,)),
            pltpu.SemaphoreType.DMA((2,)),
        ],
        compiler_params=pltpu.CompilerParams(
            collective_id=1, has_side_effects=True, vmem_limit_bytes=32 * 1024 * 1024
        ),
    )(tokens, *matrices, norm_gain, qk, trig)


def per_device(
    tokens,
    norm_gain,
    query_weight,
    key_weight,
    value_weight,
    glu_value_weight,
    glu_gate_weight,
    qk_gain,
    mix_lambda,
    head_gain,
    conv_kernel,
    channel_gain,
    channel_shift,
    output_weight,
):
    offset = lax.axis_index("sp") * 512
    positions = (offset + jnp.arange(512, dtype=jnp.int32)).astype(jnp.float32)
    inverse = 10000.0 ** (-jnp.arange(0, 32, dtype=jnp.float32) * 2.0 / 64)
    angles = inverse[:, None] * positions[None, :]
    trig = jnp.stack([jnp.cos(angles), jnp.sin(angles)])
    gains = jnp.tile(qk_gain.reshape(128), 2)
    qk = jnp.stack([gains * (64 ** (-0.5) * LOG2E), gains])[:, :, None]
    matrices = (query_weight, key_weight, value_weight, glu_value_weight, glu_gate_weight)
    own, queries, gated = project_all(tokens, matrices, norm_gain[None, :], qk, trig)
    return attend(
        own, queries, gated, mix_lambda[:, None, None], head_gain[:, None], conv_kernel,
        channel_gain[None, :], channel_shift[None, :], output_weight,
    )


def solution(mesh):
    placed = (
        P(("sp", "tp"), None),
        P(),
        P(None, "tp"),
        P(None, "tp"),
        P(None, "tp"),
        P(None, "tp"),
        P(None, "tp"),
        P(),
        P("tp"),
        P(),
        P(None, "tp"),
        P("tp"),
        P("tp"),
        P(),
    )
    return jax.shard_map(
        per_device,
        mesh=mesh,
        in_specs=placed,
        out_specs=(P(("sp", "tp"), None), P(None, "tp", "sp")),
        check_vma=False,
    )
```

time: 179 us -> 123 us (0.69)
  the two profiles are of different devices: /device:TPU:16 before, /device:TPU:63 now
where the time goes in v2:
time: 123 us
  Pallas kernels  108 us (88%)
  local copies, waits for them, and re-layouts  13.8 us (11%)
    pallas_call x1, Pallas kernels, attend(): pl.pallas_call(attend_kernel, out_shape=(jax.ShapeDtypeStruct((128, 2048)...  86.8 us
    pallas_call x1, Pallas kernels, project_all(): pl.pallas_call(project_kernel, out_shape=(jax.ShapeDtypeStruct((2, 512, 2...  21.2 us
    unnamed x22, local copies, waits for them, and re-layouts  11.4 us

profile of v2, /device:TPU:63, one launch (start us, length us, event | category | flops | bytes accessed | tf_op | source)
XLA Modules:
  0.0 122.8 jit_solution(15507222290901018283)
XLA Ops:
  0.6 0.8 tile.10
  1.4 0.7 copy.19.lam_ref
  2.2 0.8 copy.20.gain_ref
  2.9 0.3 multiply_cosine_fusion
  3.3 0.1 copy.18.qk_ref
  3.4 0.0 copy-start
  3.4 1.2 copy-done
  4.7 0.0 copy-start.1
  4.7 1.2 copy-done.1
  5.9 0.0 copy-start.2
  5.9 1.2 copy-done.2
  7.1 0.0 copy-start.3
  7.1 1.2 copy-done.3
  8.3 0.0 copy-start.4
  8.3 1.2 copy-done.4
  9.6 0.0 copy-start.5
  9.6 1.0 copy-done.5
  10.6 0.0 copy-start.7
  10.6 0.7 copy-done.7
  11.3 21.2 %shard_map.149 = (bf16[2,512,256]{2,1,0:T(8,128)(2,1)S(1)}, bf16[2,2,128,256]{3,2,1,0:T(8,128)(2,1)S(1)}, bf16[512,256]{1,0:T(8,128)(2,1)S(1)}) custom-call(bf16[128,2048]{1,0:T(8,128)(2,1)S(1)} %copy-done.5, bf16[2048,256]{1,0:T(8,128)(2,1)S(1)} %copy-done, bf16[2048,256]{1,0:T(8,128)(2,1)S(1)} %copy-done.1, bf16[2048,256]{1,0:T(8,128)(2,1)S(1)} %copy-done.2, ...), custom_call_target="tpu_custom_call" | custom-call | tf_op jit(solution)/shard_map/pallas_call | solution.py:573
  32.5 0.0 copy-start.6
  32.5 0.7 copy-done.6
  33.3 0.0 copy-start.8
  33.3 0.7 copy-done.8
  34.0 0.0 copy-start.9
  34.0 0.7 copy-done.9
  34.6 86.8 %shard_map.150 = (bf16[128,2048]{1,0:T(8,128)(2,1)S(1)}, f32[2,2,512]{2,1,0:T(2,128)S(1)}) custom-call(bf16[2,512,256]{2,1,0:T(8,128)(2,1)S(1)} %get-tuple-element.5.own_ref, bf16[2,2,128,256]{3,2,1,0:T(8,128)(2,1)S(1)} %get-tuple-element.6.query_ref, bf16[512,256]{1,0:T(8,128)(2,1)S(1)} %get-tuple-element.7.gated_ref, f32[2,1,1]{2,1,0:T(1,128)S(1)} %copy.19.lam_ref, ...), custom_call_target="tpu_custom_call" | custom-call | tf_op jit(solution)/shard_map/pallas_call | solution.py:425
  121.4 0.8 copy.23
  122.2 0.6 copy.24
  (6 shorter events, 0.0 us)
Async XLA Ops:
  3.4 1.2 %copy-start = (bf16[2048,256]{1,0:T(8,128)(2,1)S(1)}, bf16[2048,256]{1,0:T(8,128)(2,1)}, u32[]{:S(2)}) copy-start(bf16[2048,256]{1,0:T(8,128)(2,1)} %wq_ref.1) | copy-start | bytes 3145732
  4.7 1.2 copy-start.1
  5.9 1.2 copy-start.2
  7.1 1.2 copy-start.3
  8.3 1.2 copy-start.4
  9.6 1.0 copy-start.5
  10.6 0.7 copy-start.7
  32.5 0.8 copy-start.6
  33.3 0.7 copy-start.8
  34.0 0.7 copy-start.9
